TPU v7x, 128 devices: a whole 4x4x4 slice. The times are simulated.
128 devices in a mesh: sp: 64 (over z, y, x), tp: 2 (over core).
Axes of the slice: x: 4, y: 4, z: 4, core: 2. Of those that a mesh axis runs over, the one named last changes fastest.
Arguments:
- mid_rows: bfloat16 [8192, 2048], P(('sp', 'tp')), may hold values from -6 to 6
- cotangent: bfloat16 [8192, 2048], P(('sp', 'tp')), may hold values from -24 to 24
- route_experts: int32 [8192, 2], P(('sp', 'tp')), may hold values from 0 to 63, as said below
- route_weights: float32 [8192, 2], P(('sp', 'tp')), may hold values from 0.05 to 0.6
- gate_weight: bfloat16 [64, 2048, 1024], P('sp', None, 'tp'), may hold values from -0.125 to 0.125
- up_weight: bfloat16 [64, 2048, 1024], P('sp', None, 'tp'), may hold values from -0.125 to 0.125
- down_weight: bfloat16 [64, 1024, 2048], P('sp', 'tp'), may hold values from -0.1875 to 0.1875
- out_weight: bfloat16 [2048, 2048], P(None, 'tp'), may hold values from -0.125 to 0.125
- queries: bfloat16 [8192, 1024], P('sp', 'tp'), may hold values from -6 to 6
- key_rows: bfloat16 [8192, 1024], P('sp', 'tp'), may hold values from -6 to 6
- value_rows: bfloat16 [8192, 2048], P('sp', 'tp'), may hold values from -6 to 6
- log_decay: float32 [8192, 1024], P('sp', 'tp'), may hold values from -1 to 0
Outputs:
- gate_gradient: bfloat16 [64, 2048, 1024], P('sp', None, 'tp')
- up_gradient: bfloat16 [64, 2048, 1024], P('sp', None, 'tp')
- down_gradient: bfloat16 [64, 1024, 2048], P('sp', 'tp')
- out_gradient: float32 [2048, 2048], P('sp', 'tp')
- query_gradient: bfloat16 [8192, 1024], P('sp', 'tp')
- key_gradient: bfloat16 [8192, 1024], P('sp', 'tp')
- value_gradient: bfloat16 [8192, 2048], P('sp', 'tp')
- decay_gradient: float32 [8192, 1024], P('sp', 'tp')
Inputs may be any that keep to these rules, and one draw needn't show every extreme that they name: `route_experts`: each row names two different experts of one group: both lie among the same 16 consecutive numbers starting at a multiple of 16. Among the rows of one device, no expert is named more than 4 times, and one expert exactly 4 times.
All inputs are finite; a program needn't handle non-finite values.
Results may differ from a plain program's by a relative error of at most 0.0058.
Values may be sent and summed in bfloat16 or wider, within the bound.
A program may use at most 192 MiB of HBM per device.

v0:
```python
import jax
import jax.numpy as jnp
from jax import lax
from jax.experimental import pallas as pl
from jax.experimental.pallas import tpu as pltpu
from jax.sharding import Mesh
from jax.sharding import PartitionSpec as P

DK = 128
DV = 256
BLOCK = 64
SP = ("sp_0", "sp_1", "sp_2")
SP_TP = ("sp_0", "sp_1", "sp_2", "tp")


precise = lax.Precision.HIGHEST
epsilon = 1e-06
contract_rows = (((0,), (0,)), ((), ()))
contract_cols = (((1,), (1,)), ((), ()))
MESH = pl.DeviceIdType.MESH


def in_blocks(shard, dim, count):
    before, after = (shard.shape[:dim], shard.shape[dim + 1 :])
    return jnp.moveaxis(shard.reshape(*before, count, -1, *after), dim, 0)


def summed_on_arrival(shard, axis, dim):
    blocks = in_blocks(shard, dim, lax.axis_size(axis))
    arrived = lax.all_to_all(blocks, axis, split_axis=0, concat_axis=0, tiled=True)
    return arrived.astype(jnp.float32).sum(axis=0)


def neutral_like(shard, identity):
    return jax.tree.map(
        lambda a, e: jnp.broadcast_to(jnp.asarray(e, a.dtype), a.shape), shard, identity
    )


def carried_in(shard, axes, combine, identity, reverse):
    before = start = neutral_like(shard, identity)
    subtotal = shard
    for axis in reversed(axes):
        count, here = (lax.axis_size(axis), lax.axis_index(axis))
        pieces = jax.tree.map(lambda part: lax.all_gather(part, axis), subtotal)
        inside, subtotal = (start, start)
        for k in reversed(range(count)) if reverse else range(count):
            passed = k > here if reverse else k < here
            subtotal = combine(subtotal, jax.tree.map(lambda part: part[k], pieces))
            inside = jax.tree.map(lambda new, old: jnp.where(passed, new, old), subtotal, inside)
        before = combine(inside, before)
    return before


def silu_parts(pre_gate):
    gate_sigmoid = jax.nn.sigmoid(pre_gate)
    gate_swish = pre_gate * gate_sigmoid
    gate_slope = gate_sigmoid * (1.0 + pre_gate * (1.0 - gate_sigmoid))
    return (gate_swish, gate_slope)


def ring(base, step):
    return lax.rem(base + step, 4)


def rows_at(start, size):
    return pl.ds(pl.multiple_of(start, size), size)


def dot(a, b):
    return lax.dot_general(a, b, (((1,), (0,)), ((), ())), preferred_element_type=jnp.float32)


def dot_rows(a, b):
    return lax.dot_general(a, b, contract_rows, preferred_element_type=jnp.float32)


def dot_cols(a, b):
    return lax.dot_general(a, b, contract_cols, preferred_element_type=jnp.float32)


def ones_where(mask):
    return jnp.where(mask, 1.0, 0.0).astype(jnp.float32)


def bf(a):
    return a.astype(jnp.bfloat16)


def pieces_of(a):
    high = bf(a).astype(jnp.float32)
    mid = bf(a - high).astype(jnp.float32)
    return high, mid, a - high - mid


PLANE = sorted(
    [(dy, dx) for dy in range(4) for dx in range(4) if (dy, dx) != (0, 0)],
    key=lambda o: -(min(o[0], 4 - o[0]) + min(o[1], 4 - o[1])),
)
CHUNKS = 2
WIDE = 2048 // CHUNKS


def expert_kernel(
    experts_ref,
    weights_ref,
    mid_ref,
    cot_ref,
    gate_hbm,
    up_hbm,
    down_hbm,
    token_ref,
    gate_out,
    up_out,
    down_out,
    gate_w,
    up_w,
    down_w,
    z_send,
    z_note_send,
    z_recv,
    z_note,
    x_send,
    rows,
    pre_gate,
    pre_up,
    back_hidden,
    hidden,
    back_gate,
    back_up,
    half_send,
    half_recv,
    own_half,
    ret_send,
    ret_recv,
    tok_send,
    tok_recv,
    token_all,
    grad_buf,
    w_sem,
    z_ss,
    z_rs,
    n_ss,
    n_rs,
    x_ss,
    x_rs,
    d_ss,
    d_rs,
    h_ss,
    h_rs,
    r_ss,
    r_rs,
    t_ss,
    t_rs,
    a_ss,
    a_rs,
    g_sem,
):
    z, y, x, tp = [lax.axis_index(a) for a in SP_TP]
    other = 1 - tp
    here = y * 4 + x
    mine = tp * 256

    def z_peer(dz):
        return (ring(z, dz), y, x, tp)

    def plane_peer(dy, dx):
        return (z, ring(y, dy), ring(x, dx), tp)

    partner = (z, y, x, other)
    barrier = pltpu.get_barrier_semaphore()
    peers = [z_peer(dz) for dz in (1, 2, 3)] + [plane_peer(*o) for o in PLANE] + [partner]
    for peer in peers:
        pl.semaphore_signal(barrier, inc=1, device_id=peer, device_id_type=MESH)

    loads = []
    for n, (src, dst) in enumerate(((gate_hbm, gate_w), (up_hbm, up_w), (down_hbm, down_w))):
        load = pltpu.make_async_copy(src.at[0], dst, w_sem.at[n])
        load.start()
        loads.append(load)

    def remote(src, dst, ss, rs, peer):
        copy = pltpu.make_async_remote_copy(
            src_ref=src, dst_ref=dst, send_sem=ss, recv_sem=rs, device_id=peer, device_id_type=MESH
        )
        copy.start()
        return copy

    sent = []

    lane = lax.broadcasted_iota(jnp.int32, (64, 128), 1)
    first = experts_ref[:, 0:1]
    second = experts_ref[:, 1:2]
    named_first = ones_where(lane == first)
    named_second = ones_where(lane == second)
    before = bf(
        ones_where(
            lax.broadcasted_iota(jnp.int32, (64, 64), 0)
            > lax.broadcasted_iota(jnp.int32, (64, 64), 1)
        )
    )
    counts = dot(before, bf(named_first + named_second))
    rank_first = jnp.sum(named_first * counts, axis=1, keepdims=True)
    rank_second = jnp.sum(named_second * counts, axis=1, keepdims=True)
    group = lax.shift_right_logical(first, 4)
    in_group = ones_where(lane == group)
    group_rank = jnp.sum(in_group * dot(before, bf(in_group)), axis=1, keepdims=True)
    z_slot = group * 32 + group_rank.astype(jnp.int32)
    z_pick = bf(ones_where(lane == z_slot))
    slot_first = (jnp.bitwise_and(first, 15) * 16).astype(jnp.float32) + rank_first
    slot_second = (jnp.bitwise_and(second, 15) * 16).astype(jnp.float32) + rank_second
    columns = [slot_first, slot_second]
    columns += list(pieces_of(weights_ref[:, 0:1])) + list(pieces_of(weights_ref[:, 1:2]))
    note = ones_where(lane == 8)
    for n, column in enumerate(columns):
        note = jnp.where(lane == n, column, note)
    z_note_send[...] = bf(dot_rows(z_pick, bf(note)))
    for c in range(CHUNKS):
        cut = slice(c * WIDE, (c + 1) * WIDE)
        z_send[c, :, :WIDE] = bf(dot_rows(z_pick, mid_ref[:, cut]))
        z_send[c, :, WIDE:] = bf(dot_rows(z_pick, cot_ref[:, cut]))

    pl.semaphore_wait(barrier, len(peers))

    z_copies = []
    note_copies = []
    for n, dz in enumerate((2, 1, 3)):
        there = rows_at(ring(z, dz) * 32, 32)
        note_copies.append(
            remote(
                z_note_send.at[there],
                z_note.at[rows_at(z * 32, 32)],
                n_ss.at[n],
                n_rs.at[n],
                z_peer(dz),
            )
        )
    for c in range(CHUNKS):
        z_copies.append([])
        for n, dz in enumerate((2, 1, 3)):
            there = rows_at(ring(z, dz) * 32, 32)
            z_copies[c].append(
                remote(
                    z_send.at[c, there],
                    z_recv.at[c, rows_at(z * 32, 32)],
                    z_ss.at[c, n],
                    z_rs.at[c, n],
                    z_peer(dz),
                )
            )
    own_z = rows_at(z * 32, 32)
    z_note[own_z, :] = z_note_send[own_z, :]
    for c in range(CHUNKS):
        z_recv[c, own_z, :] = z_send[c, own_z, :]

    for copy in note_copies:
        copy.wait_recv()
    got = z_note[...].astype(jnp.float32)
    token_row = lax.broadcasted_iota(jnp.int32, (128, 1), 0)
    offset = lax.shift_right_logical(token_row, 5) * 4
    live = got[:, 8:9] > 0.5
    slot_a = jnp.where(live, got[:, 0:1].astype(jnp.int32) + offset, -1)
    slot_b = jnp.where(live, got[:, 1:2].astype(jnp.int32) + offset, -1)
    slot_lane = lax.broadcasted_iota(jnp.int32, (128, 256), 1)
    place_a = bf(ones_where(slot_lane == slot_a))
    place_b = bf(ones_where(slot_lane == slot_b))
    place = place_a + place_b
    weight_a = got[:, 2:3] + got[:, 3:4] + got[:, 4:5]
    weight_b = got[:, 5:6] + got[:, 6:7] + got[:, 7:8]

    x_copies = []
    own_x = rows_at(here * 16, 16)
    for c in range(CHUNKS):
        for copy in z_copies[c]:
            copy.wait_recv()
        x_send[c, :, :WIDE] = bf(dot_rows(place, z_recv[c, :, :WIDE]))
        cot_part = z_recv[c, :, WIDE:].astype(jnp.float32)
        x_send[c, :, WIDE:] = bf(
            dot_rows(place_a, bf(weight_a * cot_part)) + dot_rows(place_b, bf(weight_b * cot_part))
        )
        x_copies.append([])
        for n, (dy, dx) in enumerate(PLANE):
            there = rows_at((ring(y, dy) * 4 + ring(x, dx)) * 16, 16)
            x_copies[c].append(
                remote(
                    x_send.at[c, there],
                    rows.at[c, rows_at(mine + here * 16, 16)],
                    x_ss.at[c, n],
                    x_rs.at[c, n],
                    plane_peer(dy, dx),
                )
            )
        rows[c, rows_at(mine + here * 16, 16), :] = x_send[c, own_x, :]

    for load in loads:
        load.wait()
    for c in range(CHUNKS):
        shares = []
        for n, (dy, dx) in enumerate(((0, 0),) + tuple(PLANE)):
            if n:
                x_copies[c][n - 1].wait_recv()
            source = ring(y, 4 - dy) * 4 + ring(x, 4 - dx)
            part = rows.at[c, rows_at(mine + source * 16, 16)]
            shares.append(remote(part, part, d_ss.at[c, n], d_rs.at[c, n], partner))
        for copy in shares:
            copy.wait_recv()
        sent += shares
        cut = slice(c * WIDE, (c + 1) * WIDE)
        for ref, weight in ((pre_gate, gate_w), (pre_up, up_w)):
            value = dot(rows[c, :, :WIDE], weight[cut, :])
            ref[...] = value if c == 0 else ref[...] + value
        value = dot_cols(rows[c, :, WIDE:], down_w[:, cut])
        back_hidden[...] = value if c == 0 else back_hidden[...] + value

    gate_swish, gate_slope = silu_parts(pre_gate[...])
    hidden[...] = bf(gate_swish * pre_up[...])
    back_gate[...] = bf(back_hidden[...] * pre_up[...] * gate_slope)
    back_up[...] = bf(back_hidden[...] * gate_swish)

    half_copies = []
    their_rows = rows_at(other * 256, 256)
    own_rows = rows_at(mine, 256)
    for c in range(CHUNKS):
        cut = slice(c * WIDE, (c + 1) * WIDE)
        half_send[c] = bf(
            dot_cols(back_gate[their_rows, :], gate_w[cut, :])
            + dot_cols(back_up[their_rows, :], up_w[cut, :])
        )
        half_copies.append(
            remote(half_send.at[c], half_recv.at[c], h_ss.at[c], h_rs.at[c], partner)
        )
    r_copies = []
    for c in range(CHUNKS):
        cut = slice(c * WIDE, (c + 1) * WIDE)
        own_half[...] = bf(
            dot_cols(back_gate[own_rows, :], gate_w[cut, :])
            + dot_cols(back_up[own_rows, :], up_w[cut, :])
        )
        half_copies[c].wait_recv()
        ret_send[c] = bf(own_half[...].astype(jnp.float32) + half_recv[c].astype(jnp.float32))
        r_copies.append([])
        for n, (dy, dx) in enumerate(PLANE):
            there = rows_at((ring(y, dy) * 4 + ring(x, dx)) * 16, 16)
            r_copies[c].append(
                remote(
                    ret_send.at[c, there],
                    ret_recv.at[c, own_x],
                    r_ss.at[c, n],
                    r_rs.at[c, n],
                    plane_peer(dy, dx),
                )
            )
        ret_recv[c, own_x, :] = ret_send[c, own_x, :]
    sent += half_copies

    stores = []
    for n, (out, grad) in enumerate(((gate_out, back_gate), (up_out, back_up))):
        for c in range(CHUNKS):
            grad_buf[n, c * WIDE : (c + 1) * WIDE, :] = bf(
                dot_rows(rows[c, :, :WIDE], grad[...])
            )
        store = pltpu.make_async_copy(grad_buf.at[n], out.at[0], g_sem.at[n])
        store.start()
        stores.append(store)
    for c in range(CHUNKS):
        down_w[:, c * WIDE : (c + 1) * WIDE] = bf(dot_rows(hidden[...], rows[c, :, WIDE:]))
    store = pltpu.make_async_copy(down_w, down_out.at[0], g_sem.at[2])
    store.start()
    stores.append(store)

    t_copies = []
    for c in range(CHUNKS):
        for copy in r_copies[c]:
            copy.wait_recv()
        tok_send[c] = bf(z_recv[c, :, WIDE:].astype(jnp.float32) + dot(place, ret_recv[c]))
        t_copies.append([])
        for n, dz in enumerate((2, 1, 3)):
            there = rows_at(ring(z, dz) * 32, 32)
            t_copies[c].append(
                remote(
                    tok_send.at[c, there],
                    tok_recv.at[c, own_z],
                    t_ss.at[c, n],
                    t_rs.at[c, n],
                    z_peer(dz),
                )
            )
        tok_recv[c, own_z, :] = tok_send[c, own_z, :]
    a_copies = []
    own_tokens = rows_at(tp * 64, 64)
    for c in range(CHUNKS):
        for copy in t_copies[c]:
            copy.wait_recv()
        token_all[c, own_tokens, :] = bf(dot(z_pick, tok_recv[c]))
        part = token_all.at[c, own_tokens]
        a_copies.append(remote(part, part, a_ss.at[c], a_rs.at[c], partner))
    for c in range(CHUNKS):
        a_copies[c].wait_recv()
        token_ref[:, c * WIDE : (c + 1) * WIDE] = token_all[c]

    sent += note_copies + a_copies
    for group_of in (z_copies, x_copies, r_copies, t_copies):
        for copies in group_of:
            sent += copies
    for copy in sent:
        copy.wait_send()
    for store in stores:
        store.wait()


def expert_layer(experts, weights, mid, cot, gate, up, down):
    b16, f32 = jnp.bfloat16, jnp.float32
    v = pltpu.VMEM
    dma = pltpu.SemaphoreType.DMA
    vmem = pl.BlockSpec(memory_space=pltpu.VMEM)
    hbm = pl.BlockSpec(memory_space=pl.ANY)
    return pl.pallas_call(
        expert_kernel,
        name="expert_layer",
        out_shape=(
            jax.ShapeDtypeStruct((128, 2048), b16),
            jax.ShapeDtypeStruct((1, 2048, 512), b16),
            jax.ShapeDtypeStruct((1, 2048, 512), b16),
            jax.ShapeDtypeStruct((1, 512, 2048), b16),
        ),
        in_specs=[vmem] * 4 + [hbm] * 3,
        out_specs=(vmem, hbm, hbm, hbm),
        scratch_shapes=[
            v((2048, 512), b16),
            v((2048, 512), b16),
            v((512, 2048), b16),
            v((CHUNKS, 128, 2 * WIDE), b16),
            v((128, 128), b16),
            v((CHUNKS, 128, 2 * WIDE), b16),
            v((128, 128), b16),
            v((CHUNKS, 256, 2 * WIDE), b16),
            v((CHUNKS, 512, 2 * WIDE), b16),
            v((512, 512), f32),
            v((512, 512), f32),
            v((512, 512), f32),
            v((512, 512), b16),
            v((512, 512), b16),
            v((512, 512), b16),
            v((CHUNKS, 256, WIDE), b16),
            v((CHUNKS, 256, WIDE), b16),
            v((256, WIDE), b16),
            v((CHUNKS, 256, WIDE), b16),
            v((CHUNKS, 256, WIDE), b16),
            v((CHUNKS, 128, WIDE), b16),
            v((CHUNKS, 128, WIDE), b16),
            v((CHUNKS, 128, WIDE), b16),
            v((2, 2048, 512), b16),
            dma((3,)),
            dma((CHUNKS, 3)),
            dma((CHUNKS, 3)),
            dma((3,)),
            dma((3,)),
            dma((CHUNKS, 15)),
            dma((CHUNKS, 15)),
            dma((CHUNKS, 16)),
            dma((CHUNKS, 16)),
            dma((CHUNKS,)),
            dma((CHUNKS,)),
            dma((CHUNKS, 15)),
            dma((CHUNKS, 15)),
            dma((CHUNKS, 3)),
            dma((CHUNKS, 3)),
            dma((CHUNKS,)),
            dma((CHUNKS,)),
            dma((3,)),
        ],
        compiler_params=pltpu.CompilerParams(
            collective_id=0, has_side_effects=True, vmem_limit_bytes=60 * 1024 * 1024
        ),
        cost_estimate=pl.CostEstimate(
            flops=9_000_000_000, bytes_accessed=14_000_000, transcendentals=300_000
        ),
    )(experts, weights, mid, cot, gate, up, down)


def chain_join(earlier, later):
    return (earlier[0] * later[0], later[0][:, :, None] * earlier[1] + later[1])


def advance(carry_state, inputs):
    factor, addend = inputs
    return (factor[:, :, None] * carry_state + addend, carry_state)


def body(
    mid_rows,
    cotangent,
    route_experts,
    route_weights,
    gate_weight,
    up_weight,
    down_weight,
    out_weight,
    queries,
    key_rows,
    value_rows,
    log_decay,
):
    token_all, *totals = expert_layer(
        route_experts,
        route_weights,
        mid_rows,
        cotangent,
        gate_weight,
        up_weight,
        down_weight,
    )
    local_tokens = queries.shape[0]
    heads_local = queries.shape[1] // DK
    block_count = local_tokens // BLOCK
    query_scaled = queries.astype(jnp.float32).reshape(
        block_count, BLOCK, heads_local, DK
    ) * DK ** (-0.5)
    key_float = key_rows.astype(jnp.float32).reshape(block_count, BLOCK, heads_local, DK)
    value_float = value_rows.astype(jnp.float32).reshape(block_count, BLOCK, heads_local, DV)
    decay_float = log_decay.reshape(block_count, BLOCK, heads_local, DK)
    running_log = jnp.cumsum(decay_float, axis=1)
    block_log = running_log[:, -1]
    query_decayed = query_scaled * jnp.exp(running_log)
    key_inverse = key_float * jnp.exp(-running_log)
    end_factor = jnp.exp(block_log[:, None] - running_log)
    key_to_end = key_float * end_factor
    lower_mask = jnp.tril(jnp.ones((BLOCK, BLOCK), jnp.float32))
    scores = (
        jnp.einsum("nihc,njhc->nhij", query_decayed, key_inverse, precision=precise) * lower_mask
    )
    inner_part = jnp.einsum("nhij,njhv->nihv", scores, value_float, precision=precise)
    increment = jnp.einsum("njhc,njhv->nhcv", key_to_end, value_float, precision=precise)
    block_decay = jnp.exp(block_log)
    zero_state = jnp.zeros((heads_local, DK, DV), jnp.float32)
    local_total, local_prev = lax.scan(advance, zero_state, (block_decay, increment))
    device_decay = jnp.exp(jnp.sum(block_log, axis=0))
    prior_factor = jnp.exp(jnp.cumsum(block_log, axis=0) - block_log)
    identity = (jnp.ones_like(device_decay), jnp.zeros_like(local_total))
    carried = carried_in((device_decay, local_total), SP, chain_join, identity, False)
    incoming = carried[1]
    state_prev = local_prev + prior_factor[:, :, :, None] * incoming[None]
    state_end = device_decay[:, :, None] * incoming + local_total
    raw_out = inner_part + jnp.einsum(
        "nihc,nhcv->nihv", query_decayed, state_prev, precision=precise
    )
    inverse_root = lax.rsqrt(jnp.mean(raw_out * raw_out, axis=-1, keepdims=True) + epsilon)
    normed = raw_out * inverse_root
    normed_rows = normed.astype(jnp.bfloat16).reshape(local_tokens, heads_local * DV)
    out_total = summed_on_arrival(
        lax.dot_general(
            token_all, normed_rows, contract_rows, preferred_element_type=jnp.float32
        ).astype(jnp.bfloat16),
        SP,
        0,
    )
    back_normed = jnp.dot(token_all, out_weight, preferred_element_type=jnp.float32).reshape(
        block_count, BLOCK, heads_local, DV
    )
    back_raw = inverse_root * (
        back_normed - normed * jnp.mean(back_normed * normed, axis=-1, keepdims=True)
    )
    block_back = jnp.einsum("nihc,nihv->nhcv", query_decayed, back_raw, precision=precise)
    device_back = jnp.sum(prior_factor[:, :, :, None] * block_back, axis=0)
    later_part = carried_in((device_decay, device_back), SP, chain_join, identity, True)
    future_state = later_part[1]
    start_state, future_blocks = lax.scan(
        advance, future_state, (block_decay, block_back), reverse=True
    )
    value_dots = (
        jnp.einsum("nihv,njhv->nhij", back_raw, value_float, precision=precise) * lower_mask
    )
    query_part = jnp.einsum("nhij,njhc->nihc", value_dots, key_inverse, precision=precise)
    query_part = query_part + jnp.einsum("nihv,nhcv->nihc", back_raw, state_prev, precision=precise)
    query_back = query_part * jnp.exp(running_log)
    key_back = jnp.exp(-running_log) * jnp.einsum(
        "nhij,nihc->njhc", value_dots, query_decayed, precision=precise
    )
    key_back = key_back + end_factor * jnp.einsum(
        "nhcv,njhv->njhc", future_blocks, value_float, precision=precise
    )
    value_back = jnp.einsum("nhij,nihv->njhv", scores, back_raw, precision=precise)
    value_back = value_back + jnp.einsum(
        "njhc,nhcv->njhv", key_to_end, future_blocks, precision=precise
    )
    running_back = query_scaled * query_back - key_float * key_back
    within_block = jnp.einsum("ji,njhc->nihc", lower_mask, running_back, precision=precise)
    block_sums = jnp.sum(running_back, axis=1)
    strict_upper = jnp.triu(jnp.ones((block_count, block_count), jnp.float32), 1)
    later_blocks = jnp.einsum("nm,mhc->nhc", strict_upper, block_sums, precision=precise)
    cross_term = jnp.sum(state_end * future_state, axis=-1)
    decay_back = within_block + later_blocks[:, None] + cross_term[None, None]
    query_out = (
        (query_back * DK ** (-0.5)).astype(jnp.bfloat16).reshape(local_tokens, heads_local * DK)
    )
    key_out = key_back.astype(jnp.bfloat16).reshape(local_tokens, heads_local * DK)
    value_out = value_back.astype(jnp.bfloat16).reshape(local_tokens, heads_local * DV)
    decay_out = decay_back.reshape(local_tokens, heads_local * DK)
    return (totals[0], totals[1], totals[2], out_total, query_out, key_out, value_out, decay_out)


def solution(mesh):
    split = Mesh(mesh.devices.reshape(4, 4, 4, mesh.shape["tp"]), ("sp_0", "sp_1", "sp_2", "tp"))
    placed = (
        P(SP_TP, None),
        P(SP_TP, None),
        P(SP_TP, None),
        P(SP_TP, None),
        P(SP, None, "tp"),
        P(SP, None, "tp"),
        P(SP, "tp", None),
        P(None, "tp"),
        P(SP, "tp"),
        P(SP, "tp"),
        P(SP, "tp"),
        P(SP, "tp"),
    )
    return jax.shard_map(
        body,
        mesh=split,
        in_specs=placed,
        out_specs=(
            P(SP, None, "tp"),
            P(SP, None, "tp"),
            P(SP, "tp", None),
            P(SP, "tp"),
            P(SP, "tp"),
            P(SP, "tp"),
            P(SP, "tp"),
            P(SP, "tp"),
        ),
        check_vma=False,
    )
```

profile of v0, /device:TPU:1, one launch (start us, length us, event | category | flops | bytes accessed | tf_op | source)
XLA Modules:
  0.0 357.4 jit_solution(11410414357196489537)
XLA Ops:
  12.9 9.3 %all-gather.3 = f32[4,4,128]{2,1,0:T(4,128)S(1)} all-gather(f32[1,4,128]{2,1,0:T(4,128)S(1)} %get-tuple-element.228), channel_id=2, replica_groups=mesh['sp_0'=4,'sp_1'=4,'sp_2'=4,'tp'=2] {'sp_2'}, dimensions={0}, use_global_device_ids=true | all-gather | bytes 10240 | tf_op jit(solution)/shard_map/all_gather | solution.py:45
  22.2 9.0 %all_gather.57 = f32[4,4,128]{2,1,0:T(4,128)S(1)} all-gather(f32[1,4,128]{2,1,0:T(4,128)S(1)} %get-tuple-element.211), channel_id=1, replica_groups=mesh['sp_0'=4,'sp_1'=4,'sp_2'=4,'tp'=2] {'sp_1'}, dimensions={0}, use_global_device_ids=true | all-gather | bytes 10240 | tf_op jit(solution)/shard_map/all_gather | solution.py:45
  31.8 14.9 %all-gather.19.cloned.1.call-done = f32[16,128,256]{2,1,0:T(8,128)} async-done(((f32[4,128,256]{2,1,0:T(8,128)}), f32[16,128,256]{2,1,0:T(8,128)}) %all-gather.19.cloned.1.call-update) | async-done | bytes 2097168 | tf_op jit(solution)/shard_map/all_gather | solution.py:45
  46.7 2.7 bitcast_add_fusion.18
  49.5 8.5 %all_gather.51 = f32[4,4,128]{2,1,0:T(4,128)S(1)} all-gather(f32[1,4,128]{2,1,0:T(4,128)S(1)} %get-tuple-element.212), channel_id=1, replica_groups=mesh['sp_0'=4,'sp_1'=4,'sp_2'=4,'tp'=2] {'sp_1'}, dimensions={0}, use_global_device_ids=true | all-gather | bytes 10240 | tf_op jit(solution)/shard_map/all_gather | solution.py:45
  58.0 22.4 %all-gather.11.cloned.1.call-done = f32[4,4,128,256]{3,2,1,0:T(8,128)} async-done(((f32[1,4,128,256]{3,2,1,0:T(8,128)}), f32[4,4,128,256]{3,2,1,0:T(8,128)}) %all-gather.11.cloned.1.call-update) | async-done | bytes 2097168 | tf_op jit(solution)/shard_map/all_gather | solution.py:45
  80.4 2.6 multiply_add_fusion.4
  85.6 70.5 %expert_layer.1 = (bf16[128,2048]{1,0:T(8,128)(2,1)}, bf16[1,2048,512]{2,1,0:T(8,128)(2,1)}, bf16[1,2048,512]{2,1,0:T(8,128)(2,1)}, bf16[1,512,2048]{2,1,0:T(8,128)(2,1)}) custom-call(s32[64,2]{1,0:T(8,128)} %copy.58.experts_ref, f32[64,2]{1,0:T(8,128)} %copy.59.weights_ref, bf16[64,2048]{1,0:T(8,128)(2,1)} %mid_ref.1, bf16[64,2048]{1,0:T(8,128)(2,1)} %cot_ref.1, ...), custom_call_target="tpu_custom_call" | custom-call | flops 8999999488 | bytes 14000000 | tf_op jit(solution)/shard_map/expert_layer/pallas_call | solution.py:417
  156.2 3.9 %fusion.81 = f32[128,1024]{1,0:T(8,128)} fusion(bf16[128,2048]{1,0:T(8,128)(2,1)} %get-tuple-element.146, bf16[2048,1024]{1,0:T(8,128)(2,1)} %param.23), kind=kOutput, calls=%fused_computation.176 | convolution fusion | flops 536870912 | bytes 5242880 | tf_op jit(solution)/shard_map/dot_general | solution.py:557
  160.1 2.2 reshape.266
  162.3 8.4 %all_gather.52 = f32[4,4,128]{2,1,0:T(4,128)S(1)} all-gather(f32[1,4,128]{2,1,0:T(4,128)S(1)} %get-tuple-element.223), channel_id=1, replica_groups=mesh['sp_0'=4,'sp_1'=4,'sp_2'=4,'tp'=2] {'sp_0'}, dimensions={0}, use_global_device_ids=true | all-gather | bytes 10240 | tf_op jit(solution)/shard_map/all_gather | solution.py:45
  175.1 2.9 add_bitcast_fusion
  180.4 2.9 multiply_reduce_fusion
  183.4 32.2 %all-gather.21.cloned.1.call-done = f32[16,128,256]{2,1,0:T(8,128)} async-done(((f32[4,128,256]{2,1,0:T(8,128)}), f32[16,128,256]{2,1,0:T(8,128)}) %all-gather.21.cloned.1.call-update) | async-done | bytes 2097168 | tf_op jit(solution)/shard_map/all_gather | solution.py:45
  215.6 2.7 bitcast_add_fusion.14
  219.5 3.3 convolution_convert_fusion
  222.8 9.1 %all-to-all-start = ((bf16[64,32,1024]{2,1,0:T(8,128)(2,1)}), bf16[64,32,1024]{2,1,0:T(8,128)(2,1)}, u32[]{:S(2)}, u32[]{:S(2)}) async-start(bf16[64,32,1024]{2,1,0:T(8,128)(2,1)} %bitcast.369), calls=%async_computation | async-start | bytes 8388608 | tf_op jit(solution)/shard_map/all_to_all | solution.py:30
  232.0 65.1 %all-gather.15.cloned.1.call-done = f32[4,4,128,256]{3,2,1,0:T(8,128)} async-done(((f32[1,4,128,256]{3,2,1,0:T(8,128)}), f32[4,4,128,256]{3,2,1,0:T(8,128)}) %all-gather.15.cloned.1.call-update) | async-done | bytes 2097168 | tf_op jit(solution)/shard_map/all_gather | solution.py:45
  297.1 2.7 multiply_add_fusion.3
  299.8 8.8 %all_gather.58 = f32[4,4,128]{2,1,0:T(4,128)S(1)} all-gather(f32[1,4,128]{2,1,0:T(4,128)S(1)} %get-tuple-element.204), channel_id=1, replica_groups=mesh['sp_0'=4,'sp_1'=4,'sp_2'=4,'tp'=2] {'sp_0'}, dimensions={0}, use_global_device_ids=true | all-gather | bytes 10240 | tf_op jit(solution)/shard_map/all_gather | solution.py:45
  314.0 3.8 %convert_reduce_fusion = f32[32,1024]{1,0:T(8,128)} fusion(bf16[64,32,1024]{2,1,0:T(8,128)(2,1)} %all-to-all-done), kind=kLoop, calls=%fused_computation.6 | loop fusion | flops 4161536 | bytes 4325376 | tf_op jit(solution)/shard_map/reduce_sum | solution.py:31
  317.7 12.4 %all-gather.17.cloned.1.call-done = f32[4,4,128,256]{3,2,1,0:T(8,128)} async-done(((f32[1,4,128,256]{3,2,1,0:T(8,128)}), f32[4,4,128,256]{3,2,1,0:T(8,128)}) %all-gather.17.cloned.1.call-update) | async-done | bytes 2097168 | tf_op jit(solution)/shard_map/all_gather | solution.py:45
  330.1 5.9 %fusion.25 = (f32[4,128]{1,0:T(4,128)S(1)}, f32[4,128,256]{2,1,0:T(8,128)S(1)}) fusion(f32[4,128,256]{2,1,0:T(8,128)S(1)} %copy-done.1, f32[4,4,128,256]{3,2,1,0:T(8,128)} %all-gather.13.cloned.1.call-done, f32[4,4,128,256]{3,2,1,0:T(8,128)} %all-gather.11.cloned.1.call-done, f32[16,128,256]{2,1,0:T(8,128)S(1)} %copy-done.2, ...), kind=kLoop, calls=%fused_computation.50 | loop fusion | flops 10223104 | bytes 13688856 | tf_op jit(solution)/shard_map/reduce_sum | solution.py:591
  336.1 2.6 while.29
  (150 shorter events, 37.0 us)
Async XLA Ops:
  7.2 39.5 %all-gather.19.cloned.1.call-start = ((), (), s32[]{:S(2)}) async-start(), calls=%async_computation.5 | async-start | bytes 2621440 | tf_op jit(solution)/shard_map/all_gather | solution.py:45
  11.9 166.0 %copy-start.3 = (f32[2,4,128,256]{3,2,1,0:T(8,128)}, f32[2,4,128,256]{3,2,1,0:T(8,128)S(1)}, u32[]{:S(2)}) copy-start(f32[2,4,128,256]{3,2,1,0:T(8,128)S(1)} %get-tuple-element.147) | copy-start | bytes 3145732
  12.8 67.6 %all-gather.11.cloned.1.call-start = ((), (), s32[]{:S(2)}) async-start(), calls=%async_computation.1 | async-start | bytes 2621440 | tf_op jit(solution)/shard_map/all_gather | solution.py:45
  49.4 33.9 %copy-start.32 = (s32[64,2]{0,1:T(2,128)S(1)}, s32[64,2]{0,1:T(2,128)}, u32[]{:S(2)}) copy-start(s32[64,2]{0,1:T(2,128)} %param.18) | copy-start | bytes 1540
  49.4 34.6 %copy-start.33 = (f32[64,2]{0,1:T(2,128)S(1)}, f32[64,2]{0,1:T(2,128)}, u32[]{:S(2)}) copy-start(f32[64,2]{0,1:T(2,128)} %param.19) | copy-start | bytes 1540
  49.4 35.4 %copy-start.27 = (bf16[128,512]{1,0:T(8,128)(2,1)S(1)}, bf16[128,512]{1,0:T(8,128)(2,1)}, u32[]{:S(2)}) copy-start(bf16[128,512]{1,0:T(8,128)(2,1)} %param.24) | copy-start | bytes 393220
  49.4 125.7 %all-gather.13.cloned.1.call-start = ((), (), s32[]{:S(2)}) async-start(), calls=%async_computation.2 | async-start | bytes 2621440 | tf_op jit(solution)/shard_map/all_gather | solution.py:45
  83.1 132.5 %all-gather.21.cloned.1.call-start = ((), (), s32[]{:S(2)}) async-start(), calls=%async_computation.6 | async-start | bytes 2621440 | tf_op jit(solution)/shard_map/all_gather | solution.py:45
  160.1 15.0 %copy-start.2 = (f32[16,128,256]{2,1,0:T(8,128)S(1)}, f32[16,128,256]{2,1,0:T(8,128)}, u32[]{:S(2)}) copy-start(f32[16,128,256]{2,1,0:T(8,128)} %all-gather.19.cloned.1.call-done) | copy-start | bytes 6291460
  183.3 113.7 %all-gather.15.cloned.1.call-start = ((), (), s32[]{:S(2)}) async-start(), calls=%async_computation.3 | async-start | bytes 2621440 | tf_op jit(solution)/shard_map/all_gather | solution.py:45
  215.6 3.9 %copy-start.16 = (bf16[128,2048]{1,0:T(8,128)(2,1)S(1)}, bf16[128,2048]{1,0:T(8,128)(2,1)}, u32[]{:S(2)}) copy-start(bf16[128,2048]{1,0:T(8,128)(2,1)} %get-tuple-element.146) | copy-start | bytes 1572868
  222.8 91.1 %all-to-all-start = ((bf16[64,32,1024]{2,1,0:T(8,128)(2,1)}), bf16[64,32,1024]{2,1,0:T(8,128)(2,1)}, u32[]{:S(2)}, u32[]{:S(2)}) async-start(bf16[64,32,1024]{2,1,0:T(8,128)(2,1)} %bitcast.369), calls=%async_computation | async-start | bytes 8388608 | tf_op jit(solution)/shard_map/all_to_all | solution.py:30
  231.9 77.4 %copy-start.9 = (bf16[2,64,4,256]{3,2,1,0:T(4,128)(2,1)S(1)}, bf16[2,64,4,256]{3,2,1,0:T(4,128)(2,1)}, u32[]{:S(2)}) copy-start(bf16[2,64,4,256]{3,2,1,0:T(4,128)(2,1)} %copy-done.8) | copy-start | bytes 786436
  231.9 98.2 %all-gather.17.cloned.1.call-start = ((), (), s32[]{:S(2)}) async-start(), calls=%async_computation.4 | async-start | bytes 2621440 | tf_op jit(solution)/shard_map/all_gather | solution.py:45
  297.1 12.6 %copy-start.6 = (f32[2,64,4,128]{3,2,1,0:T(4,128)S(1)}, f32[2,64,4,128]{3,2,1,0:T(4,128)}, u32[]{:S(2)}) copy-start(f32[2,64,4,128]{3,2,1,0:T(4,128)} %copy-done.5) | copy-start | bytes 786436
  299.8 10.6 %copy-start.18 = (f32[2,4,64,64]{3,2,1,0:T(8,128)S(1)}, f32[2,4,64,64]{3,2,1,0:T(8,128)}, u32[]{:S(2)}) copy-start(f32[2,4,64,64]{3,2,1,0:T(8,128)} %copy-done.17) | copy-start | bytes 393220
  299.8 12.0 %copy-start.4 = (f32[2,4,128,256]{3,2,1,0:T(8,128)S(1)}, f32[2,4,128,256]{3,2,1,0:T(8,128)}, u32[]{:S(2)}) copy-start(f32[2,4,128,256]{3,2,1,0:T(8,128)} %copy-done.3) | copy-start | bytes 3145732
  299.8 12.0 %copy-start.15 = (f32[4,128,256]{2,1,0:T(8,128)S(1)}, f32[4,128,256]{2,1,0:T(8,128)}, u32[]{:S(2)}) copy-start(f32[4,128,256]{2,1,0:T(8,128)} %copy-done.14) | copy-start | bytes 1572868
  313.9 16.2 %copy-start.1 = (f32[4,128,256]{2,1,0:T(8,128)S(1)}, f32[4,128,256]{2,1,0:T(8,128)}, u32[]{:S(2)}) copy-start(f32[4,128,256]{2,1,0:T(8,128)} %copy-done) | copy-start | bytes 1572868
  313.9 16.2 %copy-start.28 = (f32[4,128]{1,0:T(4,128)S(1)}, f32[4,128]{1,0:T(4,128)}, u32[]{:S(2)}) copy-start(f32[4,128]{1,0:T(4,128)} %get-tuple-element.202) | copy-start | bytes 6148
  313.9 16.2 %copy-start.29 = (f32[4,128]{1,0:T(4,128)S(1)}, f32[4,128]{1,0:T(4,128)}, u32[]{:S(2)}) copy-start(f32[4,128]{1,0:T(4,128)} %get-tuple-element.203) | copy-start | bytes 6148
  313.9 16.2 %copy-start.30 = (f32[4,128]{1,0:T(4,128)S(1)}, f32[4,128]{1,0:T(4,128)}, u32[]{:S(2)}) copy-start(f32[4,128]{1,0:T(4,128)} %get-tuple-element.192) | copy-start | bytes 6148
  313.9 16.2 %copy-start.31 = (f32[4,128]{1,0:T(4,128)S(1)}, f32[4,128]{1,0:T(4,128)}, u32[]{:S(2)}) copy-start(f32[4,128]{1,0:T(4,128)} %get-tuple-element.193) | copy-start | bytes 6148
  336.1 3.4 copy-start.7
  (17 other events, 30.7 us)
Sparse Core Ops, SparseCore 0:
  12.9 33.7 all-gather.18
  49.5 30.8 all-gather.10
  83.2 39.9 all-gather.12
  183.5 32.0 all-gather.20
  218.4 78.5 all-gather.14
  299.9 30.1 all-gather.16
where the time goes:
time: 358 us; the launch traced here: 357 us
  waiting for transfers between devices  147 us (41%)
  Pallas kernels  70.5 us (20%)
  blocking collectives  43.9 us (12%)
  other arithmetic  28.6 us (8%)
  matrix products  22.4 us (6%)
  local copies, waits for them, and re-layouts  20.4 us (6%)
  between operations  14.7 us (4%)
  starting transfers between devices  9.48 us (3%)
    all_gather x6, waiting for transfers between devices, carried_in(): pieces = jax.tree.map(lambda part: lax.all_gather(part, axis), subtotal)  147 us
    pallas_call x1, Pallas kernels, expert_layer(): pl.pallas_call(expert_kernel, name='expert_layer', out_shape=(jax.ShapeDt...  70.5 us
    all_gather x5, blocking collectives, carried_in(): pieces = jax.tree.map(lambda part: lax.all_gather(part, axis), subtotal)  43.9 us
    unnamed x76, local copies, waits for them, and re-layouts  11.2 us
    add x4, other arithmetic, chain_join(): return (earlier[0] * later[0], later[0][:, :, None] * earlier[1] + later[1])  10.7 us
    all_to_all x1, starting transfers between devices, summed_on_arrival(): lax.all_to_all(blocks, axis, split_axis=0, concat_axis=0, tiled=True)  9.06 us
  transfers between devices with their start and end apart: 7, of which 5 were waited for; matrix products, arithmetic and copies ran while one was open for 8% of the time, Pallas kernels for 20%

commit v1 on v0

--- a/solution.py
+++ b/solution.py
@@ -8,48 +8,14 @@
 
 DK = 128
 DV = 256
-BLOCK = 64
 SP = ("sp_0", "sp_1", "sp_2")
 SP_TP = ("sp_0", "sp_1", "sp_2", "tp")
-
-
-precise = lax.Precision.HIGHEST
+MESH = pl.DeviceIdType.MESH
+
+
 epsilon = 1e-06
 contract_rows = (((0,), (0,)), ((), ()))
 contract_cols = (((1,), (1,)), ((), ()))
-MESH = pl.DeviceIdType.MESH
-
-
-def in_blocks(shard, dim, count):
-    before, after = (shard.shape[:dim], shard.shape[dim + 1 :])
-    return jnp.moveaxis(shard.reshape(*before, count, -1, *after), dim, 0)
-
-
-def summed_on_arrival(shard, axis, dim):
-    blocks = in_blocks(shard, dim, lax.axis_size(axis))
-    arrived = lax.all_to_all(blocks, axis, split_axis=0, concat_axis=0, tiled=True)
-    return arrived.astype(jnp.float32).sum(axis=0)
-
-
-def neutral_like(shard, identity):
-    return jax.tree.map(
-        lambda a, e: jnp.broadcast_to(jnp.asarray(e, a.dtype), a.shape), shard, identity
-    )
-
-
-def carried_in(shard, axes, combine, identity, reverse):
-    before = start = neutral_like(shard, identity)
-    subtotal = shard
-    for axis in reversed(axes):
-        count, here = (lax.axis_size(axis), lax.axis_index(axis))
-        pieces = jax.tree.map(lambda part: lax.all_gather(part, axis), subtotal)
-        inside, subtotal = (start, start)
-        for k in reversed(range(count)) if reverse else range(count):
-            passed = k > here if reverse else k < here
-            subtotal = combine(subtotal, jax.tree.map(lambda part: part[k], pieces))
-            inside = jax.tree.map(lambda new, old: jnp.where(passed, new, old), subtotal, inside)
-        before = combine(inside, before)
-    return before
 
 
 def silu_parts(pre_gate):
@@ -91,6 +57,22 @@
     high = bf(a).astype(jnp.float32)
     mid = bf(a - high).astype(jnp.float32)
     return high, mid, a - high - mid
+
+
+def split(a):
+    high = bf(a)
+    return high, bf(a - high.astype(jnp.float32))
+
+
+def twice(f, a, b):
+    high, low = split(a)
+    return f(high, b) + f(low, b)
+
+
+def thrice(f, a, b):
+    a_high, a_low = split(a)
+    b_high, b_low = split(b)
+    return f(a_high, b_high) + (f(a_high, b_low) + f(a_low, b_high))
 
 
 PLANE = sorted(
@@ -101,7 +83,7 @@
 WIDE = 2048 // CHUNKS
 
 
-def expert_kernel(
+def layer_kernel(
     experts_ref,
     weights_ref,
     mid_ref,
@@ -109,10 +91,19 @@
     gate_hbm,
     up_hbm,
     down_hbm,
-    token_ref,
+    out_w_hbm,
+    q_ref,
+    k_ref,
+    v_ref,
+    decay_ref,
     gate_out,
     up_out,
     down_out,
+    out_out,
+    q_out,
+    k_out,
+    v_out,
+    decay_out,
     gate_w,
     up_w,
     down_w,
@@ -137,6 +128,30 @@
     tok_recv,
     token_all,
     grad_buf,
+    out_w,
+    run_log,
+    q_near,
+    k_near,
+    q_start,
+    k_end,
+    scores,
+    normed,
+    root,
+    s_local,
+    s_send,
+    s_recv,
+    s_back,
+    s_in,
+    d_send,
+    d_recv,
+    n_all,
+    b_send,
+    b_recv,
+    b_back,
+    f_in,
+    tz,
+    o_send,
+    o_recv,
     w_sem,
     z_ss,
     z_rs,
@@ -155,6 +170,22 @@
     a_ss,
     a_rs,
     g_sem,
+    s_ss,
+    s_rs,
+    e_ss,
+    e_rs,
+    i_ss,
+    i_rs,
+    b_ss,
+    b_rs,
+    f_ss,
+    f_rs,
+    nz_ss,
+    nz_rs,
+    tz_ss,
+    tz_rs,
+    o_ss,
+    o_rs,
 ):
     z, y, x, tp = [lax.axis_index(a) for a in SP_TP]
     other = 1 - tp
@@ -169,13 +200,24 @@
 
     partner = (z, y, x, other)
     barrier = pltpu.get_barrier_semaphore()
-    peers = [z_peer(dz) for dz in (1, 2, 3)] + [plane_peer(*o) for o in PLANE] + [partner]
-    for peer in peers:
-        pl.semaphore_signal(barrier, inc=1, device_id=peer, device_id_type=MESH)
+    me = z * 16 + here
+
+    def far_peer(n):
+        return (ring(z, n // 16), ring(y, n // 4 % 4), ring(x, n % 4), tp)
+
+    def index_of(peer):
+        return peer[0] * 16 + peer[1] * 4 + peer[2]
+
+    def greet(n, carry):
+        pl.semaphore_signal(barrier, inc=1, device_id=far_peer(n), device_id_type=MESH)
+        return carry
+
+    lax.fori_loop(1, 64, greet, 0)
+    pl.semaphore_signal(barrier, inc=1, device_id=partner, device_id_type=MESH)
 
     loads = []
-    for n, (src, dst) in enumerate(((gate_hbm, gate_w), (up_hbm, up_w), (down_hbm, down_w))):
-        load = pltpu.make_async_copy(src.at[0], dst, w_sem.at[n])
+    for n, (src, dst) in enumerate(((gate_hbm.at[0], gate_w), (up_hbm.at[0], up_w), (down_hbm.at[0], down_w), (out_w_hbm, out_w))):
+        load = pltpu.make_async_copy(src, dst, w_sem.at[n])
         load.start()
         loads.append(load)
 
@@ -220,7 +262,7 @@
         z_send[c, :, :WIDE] = bf(dot_rows(z_pick, mid_ref[:, cut]))
         z_send[c, :, WIDE:] = bf(dot_rows(z_pick, cot_ref[:, cut]))
 
-    pl.semaphore_wait(barrier, len(peers))
+    pl.semaphore_wait(barrier, 64)
 
     z_copies = []
     note_copies = []
@@ -253,6 +295,105 @@
     for c in range(CHUNKS):
         z_recv[c, own_z, :] = z_send[c, own_z, :]
 
+    def all_to_all(make):
+        def start(n, carry):
+            for copy in make(n):
+                copy.start()
+            return carry
+
+        lax.fori_loop(1, 64, start, 0)
+
+    def arrived(make):
+        def wait(n, carry):
+            for copy in make(n):
+                copy.wait_recv()
+            return carry
+
+        lax.fori_loop(1, 64, wait, 0)
+
+    def drained(make):
+        def wait(n, carry):
+            for copy in make(n):
+                copy.wait_send()
+            return carry
+
+        lax.fori_loop(1, 64, wait, 0)
+
+    def flow(src, dst, ss, rs, n, peer):
+        return pltpu.make_async_remote_copy(
+            src_ref=src,
+            dst_ref=dst,
+            send_sem=ss.at[n],
+            recv_sem=rs.at[n],
+            device_id=peer,
+            device_id_type=MESH,
+        )
+
+    def to_scanner(send, recv, ss, rs, n):
+        peer = far_peer(n)
+        there = index_of(peer)
+        return flow(send.at[rows_at(there * 16, 16)], recv.at[me], ss, rs, n, peer)
+
+    def to_owner(back, incoming, ss, rs, n):
+        peer = far_peer(n)
+        there = index_of(peer)
+        return flow(back.at[there], incoming.at[rows_at(me * 16, 16)], ss, rs, n, peer)
+
+    def decay_flow(n):
+        peer = far_peer(n)
+        head = index_of(peer) // 16
+        return flow(d_send.at[head], d_recv.at[me], e_ss, e_rs, n, peer)
+
+    def state_out(n):
+        return (to_scanner(s_send, s_recv, s_ss, s_rs, n), decay_flow(n))
+
+    def state_in(n):
+        return (to_owner(s_back, s_in, i_ss, i_rs, n),)
+
+    def grad_out(n):
+        return (to_scanner(b_send, b_recv, b_ss, b_rs, n),)
+
+    def grad_in(n):
+        return (to_owner(b_back, f_in, f_ss, f_rs, n),)
+
+    def scan(recv, back, reverse):
+        def step(n, state):
+            at = 63 - n if reverse else n
+            back[at] = bf(state)
+            return jnp.exp(d_recv[at]) * state + recv[at].astype(jnp.float32)
+
+        lax.fori_loop(0, 64, step, jnp.zeros((16, DK), jnp.float32))
+
+    own_state = rows_at(me * 16, 16)
+    square = (128, 128)
+    at_row = lax.broadcasted_iota(jnp.int32, square, 0)
+    at_col = lax.broadcasted_iota(jnp.int32, square, 1)
+    upto = at_row >= at_col
+    lower = bf(ones_where(upto))
+    upper = bf(ones_where(at_row <= at_col))
+    high, mid, low = pieces_of(decay_ref[...])
+    run_log[...] = dot(lower, bf(high)) + dot(lower, bf(mid)) + dot(lower, bf(low))
+    for h in range(4):
+        ks = slice(h * DK, (h + 1) * DK)
+        vs = slice(h * DV, (h + 1) * DV)
+        running = run_log[:, ks]
+        middle = running[63:64]
+        total = running[127:128]
+        d_send[h] = total
+        q_scaled = q_ref[:, ks].astype(jnp.float32) * DK ** (-0.5)
+        k_float = k_ref[:, ks].astype(jnp.float32)
+        q_near[:, ks] = q_scaled * jnp.exp(running - middle)
+        k_near[:, ks] = k_float * jnp.exp(middle - running)
+        q_start[:, ks] = q_scaled * jnp.exp(running)
+        k_end[:, ks] = k_float * jnp.exp(total - running)
+        k_high, k_low = split(k_end[:, ks])
+        state = dot_rows(v_ref[:, vs], k_high) + dot_rows(v_ref[:, vs], k_low)
+        s_local[vs, :] = state
+        s_send[vs, :] = bf(state)
+    all_to_all(state_out)
+    s_recv[me] = s_send[own_state, :]
+    d_recv[me] = d_send[me // 16]
+
     for copy in note_copies:
         copy.wait_recv()
     got = z_note[...].astype(jnp.float32)
@@ -291,6 +432,28 @@
                 )
             )
         rows[c, rows_at(mine + here * 16, 16), :] = x_send[c, own_x, :]
+        if c == 0:
+            arrived(state_out)
+            scan(s_recv, s_back, False)
+            all_to_all(state_in)
+            s_in[own_state, :] = s_back[me]
+
+    for h in range(4):
+        ks = slice(h * DK, (h + 1) * DK)
+        scores[h] = jnp.where(upto, thrice(dot_cols, q_near[:, ks], k_near[:, ks]), 0.0)
+    arrived(state_in)
+    for h in range(4):
+        ks = slice(h * DK, (h + 1) * DK)
+        vs = slice(h * DV, (h + 1) * DV)
+        raw = twice(dot, scores[h], v_ref[:, vs]) + twice(dot_cols, q_start[:, ks], s_in[vs, :])
+        inverse = lax.rsqrt(jnp.mean(raw * raw, axis=-1, keepdims=True) + epsilon)
+        normed[:, vs] = raw * inverse
+        root[:, h : h + 1] = inverse
+        n_all[rows_at(z * 128, 128), vs] = bf(raw * inverse)
+    nz_copies = []
+    own_n = n_all.at[rows_at(z * 128, 128)]
+    for n, dz in enumerate((2, 1, 3)):
+        nz_copies.append(remote(own_n, own_n, nz_ss.at[n], nz_rs.at[n], z_peer(dz)))
 
     for load in loads:
         load.wait()
@@ -388,16 +551,104 @@
         tok_recv[c, own_z, :] = tok_send[c, own_z, :]
     a_copies = []
     own_tokens = rows_at(tp * 64, 64)
+    each = WIDE // 512
     for c in range(CHUNKS):
         for copy in t_copies[c]:
             copy.wait_recv()
-        token_all[c, own_tokens, :] = bf(dot(z_pick, tok_recv[c]))
-        part = token_all.at[c, own_tokens]
+        value = bf(dot(z_pick, tok_recv[c]))
+        for j in range(each):
+            token_all[c * each + j, own_tokens, :] = value[:, j * 512 : (j + 1) * 512]
+        part = token_all.at[c * each : (c + 1) * each, own_tokens]
         a_copies.append(remote(part, part, a_ss.at[c], a_rs.at[c], partner))
-    for c in range(CHUNKS):
-        a_copies[c].wait_recv()
-        token_ref[:, c * WIDE : (c + 1) * WIDE] = token_all[c]
-
+    for copy in a_copies:
+        copy.wait_recv()
+    tz_copies = []
+    for n, dz in enumerate((2, 1, 3)):
+        tz_copies.append(
+            remote(
+                token_all.at[ring(z, dz)],
+                tz.at[rows_at(z * 128, 128)],
+                tz_ss.at[n],
+                tz_rs.at[n],
+                z_peer(dz),
+            )
+        )
+    tz[rows_at(z * 128, 128), :] = token_all[z]
+
+    back_normed = dot(token_all[0], out_w[0:512, :])
+    for j in range(1, 4):
+        back_normed = back_normed + dot(token_all[j], out_w[j * 512 : (j + 1) * 512, :])
+    back_raw = []
+    for h in range(4):
+        ks = slice(h * DK, (h + 1) * DK)
+        vs = slice(h * DV, (h + 1) * DV)
+        back = back_normed[:, vs]
+        head_normed = normed[:, vs]
+        back = root[:, h : h + 1] * (
+            back - head_normed * jnp.mean(back * head_normed, axis=-1, keepdims=True)
+        )
+        normed[:, vs] = back
+        b_send[vs, :] = bf(thrice(dot_rows, back, q_start[:, ks]))
+    all_to_all(grad_out)
+    b_recv[me] = b_send[own_state, :]
+
+    for copy in tz_copies + nz_copies:
+        copy.wait_recv()
+    o_copies = []
+    o_send[...] = bf(dot_rows(tz[...], n_all[...]))
+    for n, (dy, dx) in enumerate(PLANE):
+        there = rows_at((ring(y, dy) * 4 + ring(x, dx)) * 32, 32)
+        o_copies.append(
+            remote(o_send.at[there], o_recv.at[here], o_ss.at[n], o_rs.at[n], plane_peer(dy, dx))
+        )
+    o_recv[here] = o_send[rows_at(here * 32, 32), :]
+    arrived(grad_out)
+    scan(b_recv, b_back, True)
+    all_to_all(grad_in)
+    f_in[own_state, :] = b_back[me]
+
+    for h in range(4):
+        ks = slice(h * DK, (h + 1) * DK)
+        vs = slice(h * DV, (h + 1) * DV)
+        back = normed[:, vs]
+        running = run_log[:, ks]
+        middle = running[63:64]
+        dots = jnp.where(upto, twice(dot_cols, back, v_ref[:, vs]), 0.0)
+        q_back = jnp.exp(running - middle) * thrice(dot, dots, k_near[:, ks])
+        q_back = q_back + jnp.exp(running) * twice(dot, back, s_in[vs, :])
+        k_near[:, ks] = jnp.exp(middle - running) * thrice(dot_rows, dots, q_near[:, ks])
+        normed[:, vs] = thrice(dot_rows, scores[h], back)
+        q_near[:, ks] = q_back
+        q_out[:, ks] = bf(q_back * DK ** (-0.5))
+        s_local[vs, :] = jnp.exp(running[127:128]) * s_in[vs, :].astype(jnp.float32) + s_local[vs, :]
+
+    arrived(grad_in)
+    for h in range(4):
+        ks = slice(h * DK, (h + 1) * DK)
+        vs = slice(h * DV, (h + 1) * DV)
+        running = run_log[:, ks]
+        total = running[127:128]
+        future = f_in[vs, :]
+        k_back = k_near[:, ks] + jnp.exp(total - running) * dot(v_ref[:, vs], future)
+        k_out[:, ks] = bf(k_back)
+        v_out[:, vs] = bf(normed[:, vs] + twice(dot_cols, k_end[:, ks], future))
+        cross = jnp.sum(s_local[vs, :] * future.astype(jnp.float32), axis=0, keepdims=True)
+        q_scaled = q_ref[:, ks].astype(jnp.float32) * DK ** (-0.5)
+        change = q_scaled * q_near[:, ks] - k_ref[:, ks].astype(jnp.float32) * k_back
+        high, mid, low = pieces_of(change)
+        within = dot(upper, bf(high)) + dot(upper, bf(mid)) + dot(upper, bf(low))
+        decay_out[:, ks] = within + cross
+
+    for copy in o_copies:
+        copy.wait_recv()
+    out_total = o_recv[0].astype(jnp.float32)
+    for n in range(1, 16):
+        out_total = out_total + o_recv[n].astype(jnp.float32)
+    out_out[...] = out_total
+
+    sent += nz_copies + tz_copies + o_copies
+    for make in (state_out, state_in, grad_out, grad_in):
+        drained(make)
     sent += note_copies + a_copies
     for group_of in (z_copies, x_copies, r_copies, t_copies):
         for copies in group_of:
@@ -408,33 +659,42 @@
         store.wait()
 
 
-def expert_layer(experts, weights, mid, cot, gate, up, down):
+def whole_layer(experts, weights, mid, cot, gate, up, down, out_w, queries, keys, values, decay):
     b16, f32 = jnp.bfloat16, jnp.float32
     v = pltpu.VMEM
     dma = pltpu.SemaphoreType.DMA
     vmem = pl.BlockSpec(memory_space=pltpu.VMEM)
     hbm = pl.BlockSpec(memory_space=pl.ANY)
+    wide = 2 * WIDE
+    pairs = [(CHUNKS, 3), (3,), (CHUNKS, 15), (CHUNKS, 16), (CHUNKS,), (CHUNKS, 15), (CHUNKS, 3), (CHUNKS,)]
+    sems = [dma((4,))] + [dma(shape) for shape in pairs for _ in range(2)] + [dma((3,))]
+    sems += [dma((64,)) for _ in range(10)]
+    sems += [dma(shape) for shape in ((3,), (3,), (15,)) for _ in range(2)]
     return pl.pallas_call(
-        expert_kernel,
-        name="expert_layer",
+        layer_kernel,
+        name="whole_layer",
         out_shape=(
-            jax.ShapeDtypeStruct((128, 2048), b16),
             jax.ShapeDtypeStruct((1, 2048, 512), b16),
             jax.ShapeDtypeStruct((1, 2048, 512), b16),
             jax.ShapeDtypeStruct((1, 512, 2048), b16),
+            jax.ShapeDtypeStruct((32, 1024), f32),
+            jax.ShapeDtypeStruct((128, 512), b16),
+            jax.ShapeDtypeStruct((128, 512), b16),
+            jax.ShapeDtypeStruct((128, 1024), b16),
+            jax.ShapeDtypeStruct((128, 512), f32),
         ),
-        in_specs=[vmem] * 4 + [hbm] * 3,
-        out_specs=(vmem, hbm, hbm, hbm),
+        in_specs=[vmem] * 4 + [hbm] * 4 + [vmem] * 4,
+        out_specs=(hbm, hbm, hbm, vmem, vmem, vmem, vmem, vmem),
         scratch_shapes=[
             v((2048, 512), b16),
             v((2048, 512), b16),
             v((512, 2048), b16),
-            v((CHUNKS, 128, 2 * WIDE), b16),
+            v((CHUNKS, 128, wide), b16),
             v((128, 128), b16),
-            v((CHUNKS, 128, 2 * WIDE), b16),
+            v((CHUNKS, 128, wide), b16),
             v((128, 128), b16),
-            v((CHUNKS, 256, 2 * WIDE), b16),
-            v((CHUNKS, 512, 2 * WIDE), b16),
+            v((CHUNKS, 256, wide), b16),
+            v((CHUNKS, 512, wide), b16),
             v((512, 512), f32),
             v((512, 512), f32),
             v((512, 512), f32),
@@ -448,43 +708,41 @@
             v((CHUNKS, 256, WIDE), b16),
             v((CHUNKS, 128, WIDE), b16),
             v((CHUNKS, 128, WIDE), b16),
-            v((CHUNKS, 128, WIDE), b16),
+            v((4, 128, 512), b16),
             v((2, 2048, 512), b16),
-            dma((3,)),
-            dma((CHUNKS, 3)),
-            dma((CHUNKS, 3)),
-            dma((3,)),
-            dma((3,)),
-            dma((CHUNKS, 15)),
-            dma((CHUNKS, 15)),
-            dma((CHUNKS, 16)),
-            dma((CHUNKS, 16)),
-            dma((CHUNKS,)),
-            dma((CHUNKS,)),
-            dma((CHUNKS, 15)),
-            dma((CHUNKS, 15)),
-            dma((CHUNKS, 3)),
-            dma((CHUNKS, 3)),
-            dma((CHUNKS,)),
-            dma((CHUNKS,)),
-            dma((3,)),
-        ],
+            v((2048, 1024), b16),
+            v((128, 512), f32),
+            v((128, 512), f32),
+            v((128, 512), f32),
+            v((128, 512), f32),
+            v((128, 512), f32),
+            v((4, 128, 128), f32),
+            v((128, 1024), f32),
+            v((128, 128), f32),
+            v((1024, 128), f32),
+            v((1024, 128), b16),
+            v((64, 16, 128), b16),
+            v((64, 16, 128), b16),
+            v((1024, 128), b16),
+            v((4, 1, 128), f32),
+            v((64, 1, 128), f32),
+            v((512, 1024), b16),
+            v((1024, 128), b16),
+            v((64, 16, 128), b16),
+            v((64, 16, 128), b16),
+            v((1024, 128), b16),
+            v((512, 512), b16),
+            v((512, 1024), b16),
+            v((16, 32, 1024), b16),
+        ]
+        + sems,
         compiler_params=pltpu.CompilerParams(
-            collective_id=0, has_side_effects=True, vmem_limit_bytes=60 * 1024 * 1024
+            collective_id=0, has_side_effects=True, vmem_limit_bytes=63 * 1024 * 1024
         ),
         cost_estimate=pl.CostEstimate(
-            flops=9_000_000_000, bytes_accessed=14_000_000, transcendentals=300_000
+            flops=11_000_000_000, bytes_accessed=20_000_000, transcendentals=600_000
         ),
-    )(experts, weights, mid, cot, gate, up, down)
-
-
-def chain_join(earlier, later):
-    return (earlier[0] * later[0], later[0][:, :, None] * earlier[1] + later[1])
-
-
-def advance(carry_state, inputs):
-    factor, addend = inputs
-    return (factor[:, :, None] * carry_state + addend, carry_state)
+    )(experts, weights, mid, cot, gate, up, down, out_w, queries, keys, values, decay)
 
 
 def body(
@@ -501,7 +759,7 @@
     value_rows,
     log_decay,
 ):
-    token_all, *totals = expert_layer(
+    return whole_layer(
         route_experts,
         route_weights,
         mid_rows,
@@ -509,94 +767,12 @@
         gate_weight,
         up_weight,
         down_weight,
+        out_weight,
+        queries,
+        key_rows,
+        value_rows,
+        log_decay,
     )
-    local_tokens = queries.shape[0]
-    heads_local = queries.shape[1] // DK
-    block_count = local_tokens // BLOCK
-    query_scaled = queries.astype(jnp.float32).reshape(
-        block_count, BLOCK, heads_local, DK
-    ) * DK ** (-0.5)
-    key_float = key_rows.astype(jnp.float32).reshape(block_count, BLOCK, heads_local, DK)
-    value_float = value_rows.astype(jnp.float32).reshape(block_count, BLOCK, heads_local, DV)
-    decay_float = log_decay.reshape(block_count, BLOCK, heads_local, DK)
-    running_log = jnp.cumsum(decay_float, axis=1)
-    block_log = running_log[:, -1]
-    query_decayed = query_scaled * jnp.exp(running_log)
-    key_inverse = key_float * jnp.exp(-running_log)
-    end_factor = jnp.exp(block_log[:, None] - running_log)
-    key_to_end = key_float * end_factor
-    lower_mask = jnp.tril(jnp.ones((BLOCK, BLOCK), jnp.float32))
-    scores = (
-        jnp.einsum("nihc,njhc->nhij", query_decayed, key_inverse, precision=precise) * lower_mask
-    )
-    inner_part = jnp.einsum("nhij,njhv->nihv", scores, value_float, precision=precise)
-    increment = jnp.einsum("njhc,njhv->nhcv", key_to_end, value_float, precision=precise)
-    block_decay = jnp.exp(block_log)
-    zero_state = jnp.zeros((heads_local, DK, DV), jnp.float32)
-    local_total, local_prev = lax.scan(advance, zero_state, (block_decay, increment))
-    device_decay = jnp.exp(jnp.sum(block_log, axis=0))
-    prior_factor = jnp.exp(jnp.cumsum(block_log, axis=0) - block_log)
-    identity = (jnp.ones_like(device_decay), jnp.zeros_like(local_total))
-    carried = carried_in((device_decay, local_total), SP, chain_join, identity, False)
-    incoming = carried[1]
-    state_prev = local_prev + prior_factor[:, :, :, None] * incoming[None]
-    state_end = device_decay[:, :, None] * incoming + local_total
-    raw_out = inner_part + jnp.einsum(
-        "nihc,nhcv->nihv", query_decayed, state_prev, precision=precise
-    )
-    inverse_root = lax.rsqrt(jnp.mean(raw_out * raw_out, axis=-1, keepdims=True) + epsilon)
-    normed = raw_out * inverse_root
-    normed_rows = normed.astype(jnp.bfloat16).reshape(local_tokens, heads_local * DV)
-    out_total = summed_on_arrival(
-        lax.dot_general(
-            token_all, normed_rows, contract_rows, preferred_element_type=jnp.float32
-        ).astype(jnp.bfloat16),
-        SP,
-        0,
-    )
-    back_normed = jnp.dot(token_all, out_weight, preferred_element_type=jnp.float32).reshape(
-        block_count, BLOCK, heads_local, DV
-    )
-    back_raw = inverse_root * (
-        back_normed - normed * jnp.mean(back_normed * normed, axis=-1, keepdims=True)
-    )
-    block_back = jnp.einsum("nihc,nihv->nhcv", query_decayed, back_raw, precision=precise)
-    device_back = jnp.sum(prior_factor[:, :, :, None] * block_back, axis=0)
-    later_part = carried_in((device_decay, device_back), SP, chain_join, identity, True)
-    future_state = later_part[1]
-    start_state, future_blocks = lax.scan(
-        advance, future_state, (block_decay, block_back), reverse=True
-    )
-    value_dots = (
-        jnp.einsum("nihv,njhv->nhij", back_raw, value_float, precision=precise) * lower_mask
-    )
-    query_part = jnp.einsum("nhij,njhc->nihc", value_dots, key_inverse, precision=precise)
-    query_part = query_part + jnp.einsum("nihv,nhcv->nihc", back_raw, state_prev, precision=precise)
-    query_back = query_part * jnp.exp(running_log)
-    key_back = jnp.exp(-running_log) * jnp.einsum(
-        "nhij,nihc->njhc", value_dots, query_decayed, precision=precise
-    )
-    key_back = key_back + end_factor * jnp.einsum(
-        "nhcv,njhv->njhc", future_blocks, value_float, precision=precise
-    )
-    value_back = jnp.einsum("nhij,nihv->njhv", scores, back_raw, precision=precise)
-    value_back = value_back + jnp.einsum(
-        "njhc,nhcv->njhv", key_to_end, future_blocks, precision=precise
-    )
-    running_back = query_scaled * query_back - key_float * key_back
-    within_block = jnp.einsum("ji,njhc->nihc", lower_mask, running_back, precision=precise)
-    block_sums = jnp.sum(running_back, axis=1)
-    strict_upper = jnp.triu(jnp.ones((block_count, block_count), jnp.float32), 1)
-    later_blocks = jnp.einsum("nm,mhc->nhc", strict_upper, block_sums, precision=precise)
-    cross_term = jnp.sum(state_end * future_state, axis=-1)
-    decay_back = within_block + later_blocks[:, None] + cross_term[None, None]
-    query_out = (
-        (query_back * DK ** (-0.5)).astype(jnp.bfloat16).reshape(local_tokens, heads_local * DK)
-    )
-    key_out = key_back.astype(jnp.bfloat16).reshape(local_tokens, heads_local * DK)
-    value_out = value_back.astype(jnp.bfloat16).reshape(local_tokens, heads_local * DV)
-    decay_out = decay_back.reshape(local_tokens, heads_local * DK)
-    return (totals[0], totals[1], totals[2], out_total, query_out, key_out, value_out, decay_out)
 
 
 def solution(mesh):

time: 358 us -> 138 us (0.39)
  waiting for transfers between devices: 147 us -> 0 us
  Pallas kernels: 70.5 us -> 124 us
  blocking collectives: 43.9 us -> 0 us
  other arithmetic: 28.6 us -> 0 us
  matrix products: 22.4 us -> 0 us
  between operations: 14.7 us -> 0.67 us
  starting transfers between devices: 9.48 us -> 0 us
  local copies, waits for them, and re-layouts: 20.4 us -> 13 us
    all_gather x6 -> x0, waiting for transfers between devices: 147 us -> none  [carried_in(): pieces = jax.tree.map(lambda part: lax.all_gather(part, axis), subtotal)]
    pallas_call x1, Pallas kernels: 70.5 us -> 124 us  [whole_layer(): pl.pallas_call(layer_kernel, name='whole_layer', out_shape=(jax.ShapeDtyp...]
    all_gather x5 -> x0, blocking collectives: 43.9 us -> none  [carried_in(): pieces = jax.tree.map(lambda part: lax.all_gather(part, axis), subtotal)]
    dot_general x16 -> x0, matrix products: 22.4 us -> none  [the longest x1 3.87 us: body(): jnp.dot(token_all, out_weight, preferred_element_type=jnp.float32)]
    add x8 -> x0, other arithmetic: 13.5 us -> none  [the longest x4 10.7 us: chain_join(): return (earlier[0] * later[0], later[0][:, :, None] * earlier[1] + later[1])]
    reduce_sum x4 -> x0, other arithmetic: 9.94 us -> none  [the longest x1 5.86 us: body(): cross_term = jnp.sum(state_end * future_state, axis=-1)]
    all_to_all x1 -> x0, starting transfers between devices: 9.06 us -> none  [summed_on_arrival(): lax.all_to_all(blocks, axis, split_axis=0, concat_axis=0, tiled=True)]
    reshape x5 -> x0, local copies, waits for them, and re-layouts: 6.21 us -> none  [the longest x1 2.22 us: body(): jnp.dot(token_all, out_weight, preferred_element_type=jnp.float32)]
  transfers between devices with their start and end apart: 7 -> 0, of which waited for: 5 -> 0; matrix products, arithmetic and copies ran while one was open for 8% -> 0% of each run, Pallas kernels for 20% -> 0%
where the time goes in v1:
time: 138 us; the launch traced here: 137 us
  Pallas kernels  124 us (90%)
  local copies, waits for them, and re-layouts  13 us (9%)
    pallas_call x1, Pallas kernels, whole_layer(): pl.pallas_call(layer_kernel, name='whole_layer', out_shape=(jax.ShapeDtyp...  124 us
    unnamed x24, local copies, waits for them, and re-layouts  13 us

profile of v1, /device:TPU:1, one launch (start us, length us, event | category | flops | bytes accessed | tf_op | source)
XLA Modules:
  0.0 137.5 jit_solution(3153369946196568604)
XLA Ops:
  0.6 1.4 %copy.20.experts_ref = s32[64,2]{1,0:T(8,128)} copy(s32[64,2]{0,1:T(2,128)} %param.14) | data formatting | bytes 1024 | tf_op args[2]
  2.0 1.4 %copy.21.weights_ref = f32[64,2]{1,0:T(8,128)} copy(f32[64,2]{0,1:T(2,128)} %param.15) | data formatting | bytes 1024 | tf_op args[3]
  3.4 123.8 %whole_layer.1 = (bf16[1,2048,512]{2,1,0:T(8,128)(2,1)}, bf16[1,2048,512]{2,1,0:T(8,128)(2,1)}, bf16[1,512,2048]{2,1,0:T(8,128)(2,1)}, f32[32,1024]{1,0:T(8,128)...) custom-call(s32[64,2]{1,0:T(8,128)} %copy.20.experts_ref, ...), custom_call_target="tpu_custom_call" | custom-call | flops 11000000512 | bytes 20000000 | tf_op jit(solution)/shard_map/whole_layer/pallas_call | solution.py:673
  127.2 0.0 copy-start.1
  127.2 3.2 %copy.30 = bf16[1,2048,512]{2,1,0:T(8,128)(2,1)} copy(bf16[1,2048,512]{2,1,0:T(8,128)(2,1)} %get-tuple-element.16) | data formatting | bytes 4194304
  130.4 0.0 copy-done.1
  130.4 0.0 copy-start
  130.4 1.3 copy.31
  131.7 1.0 copy-done
  132.7 0.0 copy-start.6
  132.7 0.0 copy-start.5
  132.7 0.0 copy-start.4
  132.8 0.0 copy-start.2
  132.8 1.3 copy.32
  134.1 0.0 copy-done.6
  134.1 0.7 copy.33
  134.7 0.0 copy-done.5
  134.7 0.7 copy.34
  135.4 0.0 copy-done.4
  135.4 0.7 copy.35
  136.1 0.0 copy-done.3
  136.1 0.7 copy.36
  136.8 0.0 copy-done.2
  136.8 0.7 copy.37
  (1 shorter events, 0.0 us)
Async XLA Ops:
  127.2 3.2 %copy-start.1 = (bf16[1,2048,512]{2,1,0:T(8,128)(2,1)S(1)}, bf16[1,2048,512]{2,1,0:T(8,128)(2,1)}, u32[]{:S(2)}) copy-start(bf16[1,2048,512]{2,1,0:T(8,128)(2,1)} %get-tuple-element.17) | copy-start | bytes 6291460
  130.4 2.3 %copy-start = (bf16[1,512,2048]{2,1,0:T(8,128)(2,1)S(1)}, bf16[1,512,2048]{2,1,0:T(8,128)(2,1)}, u32[]{:S(2)}) copy-start(bf16[1,512,2048]{2,1,0:T(8,128)(2,1)} %get-tuple-element.18) | copy-start | bytes 6291460
  132.7 1.3 copy-start.6
  132.7 2.0 %copy-start.5 = (bf16[128,512]{1,0:T(8,128)(2,1)S(1)}, bf16[128,512]{1,0:T(8,128)(2,1)}, u32[]{:S(2)}) copy-start(bf16[128,512]{1,0:T(8,128)(2,1)} %get-tuple-element.20) | copy-start | bytes 393220
  132.7 2.7 %copy-start.4 = (bf16[128,512]{1,0:T(8,128)(2,1)S(1)}, bf16[128,512]{1,0:T(8,128)(2,1)}, u32[]{:S(2)}) copy-start(bf16[128,512]{1,0:T(8,128)(2,1)} %get-tuple-element.21) | copy-start | bytes 393220
  132.7 3.3 %copy-start.3 = (bf16[128,1024]{1,0:T(8,128)(2,1)S(1)}, bf16[128,1024]{1,0:T(8,128)(2,1)}, u32[]{:S(2)}) copy-start(bf16[128,1024]{1,0:T(8,128)(2,1)} %get-tuple-element.22) | copy-start | bytes 786436
  132.8 4.0 %copy-start.2 = (f32[128,512]{1,0:T(8,128)S(1)}, f32[128,512]{1,0:T(8,128)}, u32[]{:S(2)}) copy-start(f32[128,512]{1,0:T(8,128)} %get-tuple-element.23) | copy-start | bytes 786436

commit v2 on v1

v2 whole, which is shorter than its diff:
```python
import jax
import jax.numpy as jnp
from jax import lax
from jax.experimental import pallas as pl
from jax.experimental.pallas import tpu as pltpu
from jax.sharding import Mesh
from jax.sharding import PartitionSpec as P

DK = 128
DV = 256
SP = ("sp_0", "sp_1", "sp_2")
SP_TP = ("sp_0", "sp_1", "sp_2", "tp")
MESH = pl.DeviceIdType.MESH


epsilon = 1e-06
contract_rows = (((0,), (0,)), ((), ()))
contract_cols = (((1,), (1,)), ((), ()))


def silu_parts(pre_gate):
    gate_sigmoid = jax.nn.sigmoid(pre_gate)
    gate_swish = pre_gate * gate_sigmoid
    gate_slope = gate_sigmoid * (1.0 + pre_gate * (1.0 - gate_sigmoid))
    return (gate_swish, gate_slope)


def ring(base, step):
    return lax.rem(base + step, 4)


def rows_at(start, size):
    return pl.ds(pl.multiple_of(start, size), size)


def dot(a, b):
    return lax.dot_general(a, b, (((1,), (0,)), ((), ())), preferred_element_type=jnp.float32)


def dot_rows(a, b):
    return lax.dot_general(a, b, contract_rows, preferred_element_type=jnp.float32)


def dot_cols(a, b):
    return lax.dot_general(a, b, contract_cols, preferred_element_type=jnp.float32)


def ones_where(mask):
    return jnp.where(mask, 1.0, 0.0).astype(jnp.float32)


def bf(a):
    return a.astype(jnp.bfloat16)


def pieces_of(a):
    high = bf(a).astype(jnp.float32)
    mid = bf(a - high).astype(jnp.float32)
    return high, mid, a - high - mid


def split(a):
    high = bf(a)
    return high, bf(a - high.astype(jnp.float32))


def twice(f, a, b):
    high, low = split(a)
    return f(high, b) + f(low, b)


def thrice(f, a, b):
    a_high, a_low = split(a)
    b_high, b_low = split(b)
    return f(a_high, b_high) + (f(a_high, b_low) + f(a_low, b_high))


PLANE = sorted(
    [(dy, dx) for dy in range(4) for dx in range(4) if (dy, dx) != (0, 0)],
    key=lambda o: -(min(o[0], 4 - o[0]) + min(o[1], 4 - o[1])),
)
CHUNKS = 4
WIDE = 2048 // CHUNKS


def layer_kernel(
    experts_ref,
    weights_ref,
    mid_hbm,
    cot_hbm,
    gate_hbm,
    up_hbm,
    down_hbm,
    out_w_hbm,
    q_hbm,
    k_hbm,
    v_hbm,
    decay_hbm,
    gate_out,
    up_out,
    down_out,
    out_out,
    q_out,
    k_out,
    v_out,
    decay_out,
    mid_ref,
    cot_ref,
    gate_w,
    up_w,
    down_w,
    out_w,
    q_ref,
    k_ref,
    v_ref,
    decay_ref,
    z_send,
    z_note_send,
    z_recv,
    z_note,
    x_send,
    rows,
    pre_gate,
    pre_up,
    back_hidden,
    hidden,
    back_gate,
    back_up,
    half_send,
    half_recv,
    ret_send,
    ret_recv,
    tok_send,
    tok_recv,
    token_all,
    run_log,
    q_near,
    k_near,
    q_start,
    k_end,
    scores,
    normed,
    root,
    s_local,
    s_send,
    s_recv,
    s_back,
    s_in,
    d_send,
    d_recv,
    d_factor,
    n_all,
    b_send,
    b_recv,
    b_back,
    f_in,
    tz,
    o_send,
    o_recv,
    w_sem,
    n_sem,
    z_sem,
    x_sem,
    d_sem,
    h_sem,
    r_sem,
    t_sem,
    a_sem,
    s_sem,
    e_sem,
    i_sem,
    b_sem,
    f_sem,
    nz_sem,
    tz_sem,
    o_sem,
):
    z, y, x, tp = [lax.axis_index(a) for a in SP_TP]
    other = 1 - tp
    here = y * 4 + x
    me = z * 16 + here
    mine = tp * 256

    def z_peer(dz):
        return (ring(z, dz), y, x, tp)

    def plane_peer(dy, dx):
        return (z, ring(y, dy), ring(x, dx), tp)

    partner = (z, y, x, other)
    barrier = pltpu.get_barrier_semaphore()
    peers = [z_peer(dz) for dz in (2, 1, 3)] + [plane_peer(*o) for o in PLANE] + [partner]
    for peer in peers:
        pl.semaphore_signal(barrier, inc=1, device_id=peer, device_id_type=MESH)

    loads = []
    moved = (
        (mid_hbm, mid_ref),
        (cot_hbm, cot_ref),
        (decay_hbm, decay_ref),
        (k_hbm, k_ref),
        (v_hbm, v_ref),
        (q_hbm, q_ref),
        (gate_hbm.at[0], gate_w),
        (up_hbm.at[0], up_w),
        (down_hbm.at[0], down_w),
        (out_w_hbm, out_w),
    )
    for n, (src, dst) in enumerate(moved):
        load = pltpu.make_async_copy(src, dst, w_sem.at[n])
        load.start()
        loads.append(load)

    def remote(src, dst, sem, peer):
        copy = pltpu.make_async_remote_copy(
            src_ref=src,
            dst_ref=dst,
            send_sem=sem.at[0],
            recv_sem=sem.at[1],
            device_id=peer,
            device_id_type=MESH,
        )
        copy.start()

    def settle(ref, sem, side):
        pltpu.make_async_copy(ref, ref, sem.at[side]).wait()

    first = experts_ref[0:1, :]
    second = experts_ref[1:2, :]
    expert_row = lax.broadcasted_iota(jnp.int32, (64, 64), 0)
    token_lane = lax.broadcasted_iota(jnp.int32, (64, 64), 1)
    named_first = ones_where(expert_row == first)
    named_second = ones_where(expert_row == second)
    before = bf(ones_where(expert_row < token_lane))
    counts = dot(bf(named_first + named_second), before)
    rank_first = jnp.sum(named_first * counts, axis=0, keepdims=True)
    rank_second = jnp.sum(named_second * counts, axis=0, keepdims=True)
    group = lax.shift_right_logical(first, 4)
    in_group = ones_where(expert_row[:16] == group)
    group_rank = jnp.sum(in_group * dot(bf(in_group), before), axis=0, keepdims=True)
    z_slot = group * 32 + group_rank.astype(jnp.int32)
    slot_row = lax.broadcasted_iota(jnp.int32, (128, 64), 0)
    z_pick = bf(ones_where(slot_row == z_slot))
    slot_first = (jnp.bitwise_and(first, 15) * 16).astype(jnp.float32) + rank_first
    slot_second = (jnp.bitwise_and(second, 15) * 16).astype(jnp.float32) + rank_second
    columns = [slot_first, slot_second]
    columns += list(pieces_of(weights_ref[0:1, :])) + list(pieces_of(weights_ref[1:2, :]))
    note = ones_where(slot_row == 8)
    for n, column in enumerate(columns):
        note = jnp.where(slot_row == n, column, note)
    z_note_send[...] = bf(dot_cols(z_pick, bf(note)))
    own_z = rows_at(z * 32, 32)
    own_x = rows_at(here * 16, 16)

    loads[0].wait()
    loads[1].wait()

    def fill_z(c):
        cut = slice(c * WIDE, (c + 1) * WIDE)
        z_send[c, :, :WIDE] = bf(dot(z_pick, mid_ref[:, cut]))
        z_send[c, :, WIDE:] = bf(dot(z_pick, cot_ref[:, cut]))

    fill_z(0)
    pl.semaphore_wait(barrier, len(peers))

    for dz in (2, 1, 3):
        there = rows_at(ring(z, dz) * 32, 32)
        remote(z_note_send.at[there], z_note.at[own_z], n_sem, z_peer(dz))
    z_note[own_z, :] = z_note_send[own_z, :]
    for c in range(CHUNKS):
        if c:
            fill_z(c)
        for dz in (2, 1, 3):
            there = rows_at(ring(z, dz) * 32, 32)
            remote(z_send.at[c, there], z_recv.at[c, own_z], z_sem.at[c], z_peer(dz))
        z_recv[c, own_z, :] = z_send[c, own_z, :]

    def far(n):
        return (ring(z, n // 16), ring(y, n // 4 % 4), ring(x, n % 4), tp)

    def all_to_all(send):
        def start(n, carry):
            peer = far(n)
            send(peer, peer[0] * 16 + peer[1] * 4 + peer[2])
            return carry

        lax.fori_loop(1, 64, start, 0)

    def state_out(peer, there):
        remote(s_send.at[rows_at(there * 16, 16)], s_recv.at[me], s_sem, peer)
        remote(d_send.at[there // 16], d_recv.at[me], e_sem, peer)

    def state_in(peer, there):
        remote(s_back.at[there], s_in.at[own_state], i_sem, peer)

    def grad_out(peer, there):
        remote(b_send.at[rows_at(there * 16, 16)], b_recv.at[me], b_sem, peer)

    def grad_in(peer, there):
        remote(b_back.at[there], f_in.at[own_state], f_sem, peer)

    def scan(recv, back, reverse):
        state = jnp.zeros((16, DK), jnp.float32)
        for n in range(64):
            at = 63 - n if reverse else n
            back[at] = bf(state)
            state = d_factor[at] * state + recv[at].astype(jnp.float32)

    own_state = rows_at(me * 16, 16)
    square = (128, 128)
    at_row = lax.broadcasted_iota(jnp.int32, square, 0)
    at_col = lax.broadcasted_iota(jnp.int32, square, 1)
    upto = at_row >= at_col
    lower = bf(ones_where(upto))
    upper = bf(ones_where(at_row <= at_col))
    for load in loads[2:6]:
        load.wait()
    high, mid, low = pieces_of(decay_ref[...])
    run_log[...] = dot(lower, bf(high)) + dot(lower, bf(mid)) + dot(lower, bf(low))
    for h in range(4):
        ks = slice(h * DK, (h + 1) * DK)
        vs = slice(h * DV, (h + 1) * DV)
        running = run_log[:, ks]
        total = running[127:128]
        d_send[h] = total
        k_end[:, ks] = k_ref[:, ks].astype(jnp.float32) * jnp.exp(total - running)
        k_high, k_low = split(k_end[:, ks])
        state = dot_rows(v_ref[:, vs], k_high) + dot_rows(v_ref[:, vs], k_low)
        s_local[vs, :] = state
        s_send[vs, :] = bf(state)

    settle(z_note.at[0:96], n_sem, 1)
    all_to_all(state_out)
    s_recv[me] = s_send[own_state, :]
    d_recv[me] = d_send[me // 16]
    got = z_note[...].astype(jnp.float32)
    token_row = lax.broadcasted_iota(jnp.int32, (128, 1), 0)
    offset = lax.shift_right_logical(token_row, 5) * 4
    live = got[:, 8:9] > 0.5
    slot_a = jnp.where(live, got[:, 0:1].astype(jnp.int32) + offset, -1)
    slot_b = jnp.where(live, got[:, 1:2].astype(jnp.int32) + offset, -1)
    slot_lane = lax.broadcasted_iota(jnp.int32, (128, 256), 1)
    place_a = bf(ones_where(slot_lane == slot_a))
    place_b = bf(ones_where(slot_lane == slot_b))
    place = place_a + place_b
    weight_a = got[:, 2:3] + got[:, 3:4] + got[:, 4:5]
    weight_b = got[:, 5:6] + got[:, 6:7] + got[:, 7:8]

    for c in range(CHUNKS):
        settle(z_recv.at[c, 0:96], z_sem.at[c], 1)
        x_send[c, :, :WIDE] = bf(dot_rows(place, z_recv[c, :, :WIDE]))
        cot_part = z_recv[c, :, WIDE:].astype(jnp.float32)
        x_send[c, :, WIDE:] = bf(
            dot_rows(place_a, bf(weight_a * cot_part)) + dot_rows(place_b, bf(weight_b * cot_part))
        )
        for dy, dx in PLANE:
            there = rows_at((ring(y, dy) * 4 + ring(x, dx)) * 16, 16)
            remote(
                x_send.at[c, there],
                rows.at[c, rows_at(mine + here * 16, 16)],
                x_sem.at[c],
                plane_peer(dy, dx),
            )
        rows[c, rows_at(mine + here * 16, 16), :] = x_send[c, own_x, :]
        if c == 1:
            settle(s_recv.at[0:63], s_sem, 1)
            settle(d_recv.at[0:63], e_sem, 1)
            d_factor[...] = jnp.exp(d_recv[...])
            scan(s_recv, s_back, False)
            all_to_all(state_in)
            s_in[own_state, :] = s_back[me]

    for h in range(4):
        ks = slice(h * DK, (h + 1) * DK)
        running = run_log[:, ks]
        middle = running[63:64]
        q_scaled = q_ref[:, ks].astype(jnp.float32) * DK ** (-0.5)
        q_near[:, ks] = q_scaled * jnp.exp(running - middle)
        k_near[:, ks] = k_ref[:, ks].astype(jnp.float32) * jnp.exp(middle - running)
        q_start[:, ks] = q_scaled * jnp.exp(running)
        scores[h] = jnp.where(upto, thrice(dot_cols, q_near[:, ks], k_near[:, ks]), 0.0)
    settle(s_in.at[0:1008], i_sem, 1)
    for h in range(4):
        ks = slice(h * DK, (h + 1) * DK)
        vs = slice(h * DV, (h + 1) * DV)
        raw = twice(dot, scores[h], v_ref[:, vs]) + twice(dot_cols, q_start[:, ks], s_in[vs, :])
        inverse = lax.rsqrt(jnp.mean(raw * raw, axis=-1, keepdims=True) + epsilon)
        normed[:, vs] = raw * inverse
        root[:, h : h + 1] = inverse
        n_all[rows_at(z * 128, 128), vs] = bf(raw * inverse)
    own_n = n_all.at[rows_at(z * 128, 128)]
    for dz in (2, 1, 3):
        remote(own_n, own_n, nz_sem, z_peer(dz))

    for load in loads[6:]:
        load.wait()
    their_rows = rows_at(other * 256, 256)
    own_rows = rows_at(mine, 256)

    def gather_up(c, part):
        cut = slice(c * WIDE, (c + 1) * WIDE)
        for ref, value in (
            (pre_gate, dot(rows[c, part, :WIDE], gate_w[cut, :])),
            (pre_up, dot(rows[c, part, :WIDE], up_w[cut, :])),
            (back_hidden, dot_cols(rows[c, part, WIDE:], down_w[:, cut])),
        ):
            ref[part, :] = value if c == 0 else ref[part, :] + value

    for c in range(CHUNKS):
        settle(rows.at[c, 0:240], x_sem.at[c], 1)
        remote(rows.at[c, own_rows], rows.at[c, own_rows], d_sem.at[c], partner)
        gather_up(c, own_rows)
        settle(rows.at[c, 0:256], d_sem.at[c], 1)
        gather_up(c, their_rows)

    gate_swish, gate_slope = silu_parts(pre_gate[...])
    hidden[...] = bf(gate_swish * pre_up[...])
    back_gate[...] = bf(back_hidden[...] * pre_up[...] * gate_slope)
    back_up[...] = bf(back_hidden[...] * gate_swish)

    def half_of(part, c):
        cut = slice(c * WIDE, (c + 1) * WIDE)
        return bf(
            dot_cols(back_gate[part, :], gate_w[cut, :]) + dot_cols(back_up[part, :], up_w[cut, :])
        )

    def send_half(c):
        half_send[c] = half_of(their_rows, c)
        remote(half_send.at[c], half_recv.at[c], h_sem.at[c], partner)

    def give_back(c):
        own_half = half_of(own_rows, c).astype(jnp.float32)
        settle(half_recv.at[c], h_sem.at[c], 1)
        ret_send[c] = bf(own_half + half_recv[c].astype(jnp.float32))
        for dy, dx in PLANE:
            there = rows_at((ring(y, dy) * 4 + ring(x, dx)) * 16, 16)
            remote(ret_send.at[c, there], ret_recv.at[c, own_x], r_sem.at[c], plane_peer(dy, dx))
        ret_recv[c, own_x, :] = ret_send[c, own_x, :]

    send_half(0)
    for c in range(CHUNKS):
        if c + 1 < CHUNKS:
            send_half(c + 1)
        give_back(c)

    for c in range(CHUNKS):
        cut = slice(c * WIDE, (c + 1) * WIDE)
        gate_out[0, cut, :] = bf(dot_rows(rows[c, :, :WIDE], back_gate[...]))
        up_out[0, cut, :] = bf(dot_rows(rows[c, :, :WIDE], back_up[...]))
        down_out[0, :, cut] = bf(dot_rows(hidden[...], rows[c, :, WIDE:]))

    own_tokens = rows_at(tp * 64, 64)

    def to_tokens(c):
        settle(ret_recv.at[c, 0:240], r_sem.at[c], 1)
        tok_send[c] = bf(z_recv[c, :, WIDE:].astype(jnp.float32) + dot(place, ret_recv[c]))
        for dz in (2, 1, 3):
            there = rows_at(ring(z, dz) * 32, 32)
            remote(tok_send.at[c, there], tok_recv.at[c, own_z], t_sem.at[c], z_peer(dz))
        tok_recv[c, own_z, :] = tok_send[c, own_z, :]

    def share_tokens(c):
        settle(tok_recv.at[c, 0:96], t_sem.at[c], 1)
        token_all[c, own_tokens, :] = bf(dot_rows(z_pick, tok_recv[c]))
        part = token_all.at[c, own_tokens]
        remote(part, part, a_sem.at[c], partner)

    def use_tokens(c, total):
        settle(token_all.at[c, 0:64], a_sem.at[c], 1)

        @pl.when(z != c)
        def send():
            remote(token_all.at[c], tz.at[rows_at(z * 128, 128)], tz_sem, (c, y, x, tp))

        value = dot(token_all[c], out_w[c * WIDE : (c + 1) * WIDE, :])
        return value if total is None else total + value

    to_tokens(0)
    to_tokens(1)
    share_tokens(0)
    to_tokens(2)
    share_tokens(1)
    back_normed = use_tokens(0, None)
    to_tokens(3)
    share_tokens(2)
    back_normed = use_tokens(1, back_normed)
    share_tokens(3)
    back_normed = use_tokens(2, back_normed)
    back_normed = use_tokens(3, back_normed)

    for h in range(4):
        ks = slice(h * DK, (h + 1) * DK)
        vs = slice(h * DV, (h + 1) * DV)
        back = back_normed[:, vs]
        head_normed = normed[:, vs]
        back = root[:, h : h + 1] * (
            back - head_normed * jnp.mean(back * head_normed, axis=-1, keepdims=True)
        )
        normed[:, vs] = back
        b_send[vs, :] = bf(thrice(dot_rows, back, q_start[:, ks]))
    all_to_all(grad_out)
    b_recv[me] = b_send[own_state, :]

    tz[rows_at(z * 128, 128), :] = token_all[z]
    settle(tz.at[0:384], tz_sem, 1)
    settle(n_all.at[0:384], nz_sem, 1)
    o_send[...] = bf(dot_rows(tz[...], n_all[...]))

    def spread(offsets):
        for dy, dx in offsets:
            there = rows_at((ring(y, dy) * 4 + ring(x, dx)) * 32, 32)
            remote(o_send.at[there], o_recv.at[here], o_sem, plane_peer(dy, dx))

    spread(PLANE[:7])
    o_recv[here] = o_send[rows_at(here * 32, 32), :]
    settle(b_recv.at[0:63], b_sem, 1)
    scan(b_recv, b_back, True)
    all_to_all(grad_in)
    f_in[own_state, :] = b_back[me]
    spread(PLANE[7:])

    for h in range(4):
        ks = slice(h * DK, (h + 1) * DK)
        vs = slice(h * DV, (h + 1) * DV)
        back = normed[:, vs]
        running = run_log[:, ks]
        middle = running[63:64]
        dots = jnp.where(upto, twice(dot_cols, back, v_ref[:, vs]), 0.0)
        q_back = jnp.exp(running - middle) * thrice(dot, dots, k_near[:, ks])
        q_back = q_back + jnp.exp(running) * twice(dot, back, s_in[vs, :])
        k_near[:, ks] = jnp.exp(middle - running) * thrice(dot_rows, dots, q_near[:, ks])
        normed[:, vs] = thrice(dot_rows, scores[h], back)
        q_near[:, ks] = q_back
        q_out[:, ks] = bf(q_back * DK ** (-0.5))
        s_local[vs, :] = jnp.exp(running[127:128]) * s_in[vs, :].astype(jnp.float32) + s_local[vs, :]

    settle(z_note_send.at[0:96], n_sem, 0)
    settle(s_send.at[0:1008], s_sem, 0)
    settle(d_recv.at[0:63], e_sem, 0)
    settle(s_back.at[0:63], i_sem, 0)
    settle(n_all.at[0:384], nz_sem, 0)
    settle(tz.at[0:384], tz_sem, 0)
    settle(b_send.at[0:1008], b_sem, 0)
    for c in range(CHUNKS):
        settle(z_send.at[c, 0:96], z_sem.at[c], 0)
        settle(x_send.at[c, 0:240], x_sem.at[c], 0)
        settle(rows.at[c, 0:256], d_sem.at[c], 0)
        settle(half_send.at[c], h_sem.at[c], 0)
        settle(ret_send.at[c, 0:240], r_sem.at[c], 0)
        settle(tok_send.at[c, 0:96], t_sem.at[c], 0)
        settle(token_all.at[c, 0:64], a_sem.at[c], 0)
    settle(f_in.at[0:1008], f_sem, 1)
    for h in range(4):
        ks = slice(h * DK, (h + 1) * DK)
        vs = slice(h * DV, (h + 1) * DV)
        running = run_log[:, ks]
        total = running[127:128]
        future = f_in[vs, :]
        k_back = k_near[:, ks] + jnp.exp(total - running) * dot(v_ref[:, vs], future)
        k_out[:, ks] = bf(k_back)
        v_out[:, vs] = bf(normed[:, vs] + twice(dot_cols, k_end[:, ks], future))
        cross = jnp.sum(s_local[vs, :] * future.astype(jnp.float32), axis=0, keepdims=True)
        q_scaled = q_ref[:, ks].astype(jnp.float32) * DK ** (-0.5)
        change = q_scaled * q_near[:, ks] - k_ref[:, ks].astype(jnp.float32) * k_back
        high, mid, low = pieces_of(change)
        within = dot(upper, bf(high)) + dot(upper, bf(mid)) + dot(upper, bf(low))
        decay_out[:, ks] = within + cross

    settle(o_recv.at[0:15], o_sem, 1)
    out_total = o_recv[0].astype(jnp.float32)
    for n in range(1, 16):
        out_total = out_total + o_recv[n].astype(jnp.float32)
    out_out[...] = out_total
    settle(o_recv.at[0:15], o_sem, 0)
    settle(b_back.at[0:63], f_sem, 0)


def finish_kernel(*refs):
    count = len(refs) // 2
    sems = refs[-1]
    copies = []
    for n in range(count):
        copy = pltpu.make_async_copy(refs[n], refs[count + n], sems.at[n])
        copy.start()
        copies.append(copy)
    for copy in copies:
        copy.wait()


def whole_layer(experts, weights, mid, cot, gate, up, down, out_w, queries, keys, values, decay):
    b16, f32 = jnp.bfloat16, jnp.float32
    v = pltpu.VMEM
    dma = pltpu.SemaphoreType.DMA
    vmem = pl.BlockSpec(memory_space=pltpu.VMEM)
    hbm = pl.BlockSpec(memory_space=pl.ANY)
    outs = (
        ((1, 2048, 512), b16),
        ((1, 2048, 512), b16),
        ((1, 512, 2048), b16),
        ((32, 1024), f32),
        ((128, 512), b16),
        ((128, 512), b16),
        ((128, 1024), b16),
        ((128, 512), f32),
    )
    scratch = (
        ((64, 2048), b16),
        ((64, 2048), b16),
        ((2048, 512), b16),
        ((2048, 512), b16),
        ((512, 2048), b16),
        ((2048, 1024), b16),
        ((128, 512), b16),
        ((128, 512), b16),
        ((128, 1024), b16),
        ((128, 512), f32),
        ((CHUNKS, 128, 2 * WIDE), b16),
        ((128, 128), b16),
        ((CHUNKS, 128, 2 * WIDE), b16),
        ((128, 128), b16),
        ((CHUNKS, 256, 2 * WIDE), b16),
        ((CHUNKS, 512, 2 * WIDE), b16),
        ((512, 512), f32),
        ((512, 512), f32),
        ((512, 512), f32),
        ((512, 512), b16),
        ((512, 512), b16),
        ((512, 512), b16),
        ((CHUNKS, 256, WIDE), b16),
        ((CHUNKS, 256, WIDE), b16),
        ((CHUNKS, 256, WIDE), b16),
        ((CHUNKS, 256, WIDE), b16),
        ((CHUNKS, 128, WIDE), b16),
        ((CHUNKS, 128, WIDE), b16),
        ((4, 128, 512), b16),
        ((128, 512), f32),
        ((128, 512), f32),
        ((128, 512), f32),
        ((128, 512), f32),
        ((128, 512), f32),
        ((4, 128, 128), f32),
        ((128, 1024), f32),
        ((128, 128), f32),
        ((1024, 128), f32),
        ((1024, 128), b16),
        ((64, 16, 128), b16),
        ((64, 16, 128), b16),
        ((1024, 128), b16),
        ((4, 1, 128), f32),
        ((64, 1, 128), f32),
        ((64, 1, 128), f32),
        ((512, 1024), b16),
        ((1024, 128), b16),
        ((64, 16, 128), b16),
        ((64, 16, 128), b16),
        ((1024, 128), b16),
        ((512, 512), b16),
        ((512, 1024), b16),
        ((16, 32, 1024), b16),
    )
    two, many = (2,), (CHUNKS, 2)
    sems = [(10,), two] + [many] * 7 + [two] * 8
    made = pl.pallas_call(
        layer_kernel,
        name="whole_layer",
        out_shape=tuple(v(shape, kind) for shape, kind in outs),
        in_specs=[vmem] * 2 + [hbm] * 10,
        out_specs=(vmem,) * 8,
        scratch_shapes=[v(shape, kind) for shape, kind in scratch] + [dma(shape) for shape in sems],
        compiler_params=pltpu.CompilerParams(
            collective_id=0, has_side_effects=True, vmem_limit_bytes=50 * 1024 * 1024
        ),
        cost_estimate=pl.CostEstimate(
            flops=11_000_000_000, bytes_accessed=20_000_000, transcendentals=600_000
        ),
    )(experts.T, weights.T, mid, cot, gate, up, down, out_w, queries, keys, values, decay)
    return pl.pallas_call(
        finish_kernel,
        name="finish",
        out_shape=tuple(jax.ShapeDtypeStruct(shape, kind) for shape, kind in outs),
        in_specs=[vmem] * 8,
        out_specs=(hbm,) * 8,
        scratch_shapes=[dma((8,))],
        compiler_params=pltpu.CompilerParams(vmem_limit_bytes=1024 * 1024),
    )(*[pltpu.with_memory_space_constraint(a, pltpu.VMEM) for a in made])


def body(
    mid_rows,
    cotangent,
    route_experts,
    route_weights,
    gate_weight,
    up_weight,
    down_weight,
    out_weight,
    queries,
    key_rows,
    value_rows,
    log_decay,
):
    return whole_layer(
        route_experts,
        route_weights,
        mid_rows,
        cotangent,
        gate_weight,
        up_weight,
        down_weight,
        out_weight,
        queries,
        key_rows,
        value_rows,
        log_decay,
    )


def solution(mesh):
    split = Mesh(mesh.devices.reshape(4, 4, 4, mesh.shape["tp"]), ("sp_0", "sp_1", "sp_2", "tp"))
    placed = (
        P(SP_TP, None),
        P(SP_TP, None),
        P(SP_TP, None),
        P(SP_TP, None),
        P(SP, None, "tp"),
        P(SP, None, "tp"),
        P(SP, "tp", None),
        P(None, "tp"),
        P(SP, "tp"),
        P(SP, "tp"),
        P(SP, "tp"),
        P(SP, "tp"),
    )
    return jax.shard_map(
        body,
        mesh=split,
        in_specs=placed,
        out_specs=(
            P(SP, None, "tp"),
            P(SP, None, "tp"),
            P(SP, "tp", None),
            P(SP, "tp"),
            P(SP, "tp"),
            P(SP, "tp"),
            P(SP, "tp"),
            P(SP, "tp"),
        ),
        check_vma=False,
    )
```

time: 138 us -> 102 us (0.74)
  Pallas kernels: 124 us -> 101 us
  local copies, waits for them, and re-layouts: 13 us -> 0 us
    pallas_call x1 -> x2, Pallas kernels: 124 us -> 101 us  [the longest x1 98.2 us: whole_layer(): pl.pallas_call(layer_kernel, name='whole_layer', out_shape=tuple((v(shape...]
    unnamed x24 -> x0, local copies, waits for them, and re-layouts: 13 us -> none
where the time goes in v2:
time: 102 us
  Pallas kernels  101 us (99%)
    pallas_call x1, Pallas kernels, whole_layer(): pl.pallas_call(layer_kernel, name='whole_layer', out_shape=tuple((v(shape...  98.2 us
    pallas_call x1, Pallas kernels, whole_layer(): pl.pallas_call(finish_kernel, name='finish', out_shape=tuple((jax.ShapeDt...  2.98 us

profile of v2, /device:TPU:1, one launch (start us, length us, event | category | flops | bytes accessed | tf_op | source)
XLA Modules:
  0.0 101.9 jit_solution(10489966254731477461)
XLA Ops:
  0.6 98.2 %whole_layer.1 = (bf16[1,2048,512]{2,1,0:T(8,128)(2,1)S(1)}, bf16[1,2048,512]{2,1,0:T(8,128)(2,1)S(1)}, bf16[1,512,2048]{2,1,0:T(8,128)(2,1)S(1)}, f32[32,1024]{...) custom-call(s32[2,64]{1,0:T(2,128)} %bitcast.2, ...), custom_call_target="tpu_custom_call" | custom-call | flops 11000000512 | bytes 20000000 | tf_op jit(solution)/shard_map/whole_layer/pallas_call | solution.py:663
  98.8 3.0 %finish.1 = (bf16[1,2048,512]{2,1,0:T(8,128)(2,1)}, bf16[1,2048,512]{2,1,0:T(8,128)(2,1)}, bf16[1,512,2048]{2,1,0:T(8,128)(2,1)}, f32[32,1024]{1,0:T(8,128)}, bf...) custom-call(bf16[1,2048,512]{2,1,0:T(8,128)(2,1)S(1)} %get-tuple-element.16.r, ...), custom_call_target="tpu_custom_call" | custom-call | tf_op jit(solution)/shard_map/finish/pallas_call | solution.py:677

commit v3 on v2

--- a/solution.py
+++ b/solution.py
@@ -53,6 +53,11 @@
     return a.astype(jnp.bfloat16)
 
 
+def total_of(parts):
+    total = parts[0].astype(jnp.float32) + parts[1].astype(jnp.float32)
+    return total + parts[2].astype(jnp.float32) + parts[3].astype(jnp.float32)
+
+
 def pieces_of(a):
     high = bf(a).astype(jnp.float32)
     mid = bf(a - high).astype(jnp.float32)
@@ -78,6 +83,10 @@
 PLANE = sorted(
     [(dy, dx) for dy in range(4) for dx in range(4) if (dy, dx) != (0, 0)],
     key=lambda o: -(min(o[0], 4 - o[0]) + min(o[1], 4 - o[1])),
+)
+FAR = sorted(
+    [(i, j, k) for i in range(4) for j in range(4) for k in range(4) if i + j + k],
+    key=lambda o: -sum(min(d, 4 - d) for d in o),
 )
 CHUNKS = 4
 WIDE = 2048 // CHUNKS
@@ -157,6 +166,12 @@
     tz,
     o_send,
     o_recv,
+    o_part,
+    o_last,
+    p_send,
+    p_recv,
+    p_part,
+    p_last,
     w_sem,
     n_sem,
     z_sem,
@@ -173,7 +188,11 @@
     f_sem,
     nz_sem,
     tz_sem,
+    tz2_sem,
     o_sem,
+    o2_sem,
+    p_sem,
+    p2_sem,
 ):
     z, y, x, tp = [lax.axis_index(a) for a in SP_TP]
     other = 1 - tp
@@ -267,24 +286,22 @@
         there = rows_at(ring(z, dz) * 32, 32)
         remote(z_note_send.at[there], z_note.at[own_z], n_sem, z_peer(dz))
     z_note[own_z, :] = z_note_send[own_z, :]
-    for c in range(CHUNKS):
-        if c:
-            fill_z(c)
+
+    def send_z(c):
         for dz in (2, 1, 3):
             there = rows_at(ring(z, dz) * 32, 32)
             remote(z_send.at[c, there], z_recv.at[c, own_z], z_sem.at[c], z_peer(dz))
         z_recv[c, own_z, :] = z_send[c, own_z, :]
 
-    def far(n):
-        return (ring(z, n // 16), ring(y, n // 4 % 4), ring(x, n % 4), tp)
+    send_z(0)
+
+    along_z, along_y, along_x = [[ring(a, d) for d in range(4)] for a in (z, y, x)]
+    bases = [[along_z[i] * 16 + along_y[j] * 4 for j in range(4)] for i in range(4)]
 
     def all_to_all(send):
-        def start(n, carry):
-            peer = far(n)
-            send(peer, peer[0] * 16 + peer[1] * 4 + peer[2])
-            return carry
-
-        lax.fori_loop(1, 64, start, 0)
+        for i, j, k in FAR:
+            peer = (along_z[i], along_y[j], along_x[k], tp)
+            send(peer, bases[i][j] + along_x[k])
 
     def state_out(peer, there):
         remote(s_send.at[rows_at(there * 16, 16)], s_recv.at[me], s_sem, peer)
@@ -333,6 +350,9 @@
     all_to_all(state_out)
     s_recv[me] = s_send[own_state, :]
     d_recv[me] = d_send[me // 16]
+    for c in range(1, CHUNKS):
+        fill_z(c)
+        send_z(c)
     got = z_note[...].astype(jnp.float32)
     token_row = lax.broadcasted_iota(jnp.int32, (128, 1), 0)
     offset = lax.shift_right_logical(token_row, 5) * 4
@@ -465,13 +485,12 @@
         part = token_all.at[c, own_tokens]
         remote(part, part, a_sem.at[c], partner)
 
+        @pl.when(z != c)
+        def send():
+            remote(part, tz.at[rows_at(z * 128 + tp * 64, 64)], tz_sem, (c, y, x, tp))
+
     def use_tokens(c, total):
         settle(token_all.at[c, 0:64], a_sem.at[c], 1)
-
-        @pl.when(z != c)
-        def send():
-            remote(token_all.at[c], tz.at[rows_at(z * 128, 128)], tz_sem, (c, y, x, tp))
-
         value = dot(token_all[c], out_w[c * WIDE : (c + 1) * WIDE, :])
         return value if total is None else total + value
 
@@ -480,9 +499,9 @@
     share_tokens(0)
     to_tokens(2)
     share_tokens(1)
-    back_normed = use_tokens(0, None)
     to_tokens(3)
     share_tokens(2)
+    back_normed = use_tokens(0, None)
     back_normed = use_tokens(1, back_normed)
     share_tokens(3)
     back_normed = use_tokens(2, back_normed)
@@ -502,22 +521,30 @@
     b_recv[me] = b_send[own_state, :]
 
     tz[rows_at(z * 128, 128), :] = token_all[z]
-    settle(tz.at[0:384], tz_sem, 1)
+    settle(tz.at[0:192], tz_sem, 1)
+    for d in (1, 2, 3):
+        part = tz.at[rows_at(along_z[d] * 128 + tp * 64, 64)]
+        remote(part, part, tz2_sem, partner)
+    settle(tz.at[0:192], tz2_sem, 1)
     settle(n_all.at[0:384], nz_sem, 1)
-    o_send[...] = bf(dot_rows(tz[...], n_all[...]))
-
-    def spread(offsets):
-        for dy, dx in offsets:
-            there = rows_at((ring(y, dy) * 4 + ring(x, dx)) * 32, 32)
-            remote(o_send.at[there], o_recv.at[here], o_sem, plane_peer(dy, dx))
-
-    spread(PLANE[:7])
-    o_recv[here] = o_send[rows_at(here * 32, 32), :]
+    o_send[...] = bf(dot_rows(tz[...], n_all[:, :512]))
+    for d in (2, 1, 3):
+        there = rows_at(along_y[d] * 128, 128)
+        remote(o_send.at[there], o_recv.at[y], o_sem, (z, along_y[d], x, tp))
+    o_recv[y] = o_send[rows_at(y * 128, 128), :]
+    p_send[...] = bf(dot_rows(tz[...], n_all[:, 512:]))
+    for d in (2, 1, 3):
+        for j in range(4):
+            there = rows_at(along_x[d] * 32 + j * 128, 32)
+            remote(
+                p_send.at[there], p_recv.at[x, j * 32 : (j + 1) * 32], p_sem, (z, y, along_x[d], tp)
+            )
+    for j in range(4):
+        p_recv[x, j * 32 : (j + 1) * 32, :] = p_send[rows_at(x * 32 + j * 128, 32), :]
     settle(b_recv.at[0:63], b_sem, 1)
     scan(b_recv, b_back, True)
     all_to_all(grad_in)
     f_in[own_state, :] = b_back[me]
-    spread(PLANE[7:])
 
     for h in range(4):
         ks = slice(h * DK, (h + 1) * DK)
@@ -534,12 +561,25 @@
         q_out[:, ks] = bf(q_back * DK ** (-0.5))
         s_local[vs, :] = jnp.exp(running[127:128]) * s_in[vs, :].astype(jnp.float32) + s_local[vs, :]
 
+    settle(o_recv.at[0:3], o_sem, 1)
+    o_part[...] = bf(total_of(o_recv))
+    for d in (2, 1, 3):
+        there = rows_at(along_x[d] * 32, 32)
+        remote(o_part.at[there], o_last.at[x], o2_sem, (z, y, along_x[d], tp))
+    o_last[x] = o_part[rows_at(x * 32, 32), :]
+    settle(p_recv.at[0:3], p_sem, 1)
+    p_part[...] = bf(total_of(p_recv))
+    for d in (2, 1, 3):
+        there = rows_at(along_y[d] * 32, 32)
+        remote(p_part.at[there], p_last.at[y], p2_sem, (z, along_y[d], x, tp))
+    p_last[y] = p_part[rows_at(y * 32, 32), :]
     settle(z_note_send.at[0:96], n_sem, 0)
     settle(s_send.at[0:1008], s_sem, 0)
     settle(d_recv.at[0:63], e_sem, 0)
     settle(s_back.at[0:63], i_sem, 0)
     settle(n_all.at[0:384], nz_sem, 0)
-    settle(tz.at[0:384], tz_sem, 0)
+    settle(tz.at[0:192], tz_sem, 0)
+    settle(tz.at[0:192], tz2_sem, 0)
     settle(b_send.at[0:1008], b_sem, 0)
     for c in range(CHUNKS):
         settle(z_send.at[c, 0:96], z_sem.at[c], 0)
@@ -566,12 +606,14 @@
         within = dot(upper, bf(high)) + dot(upper, bf(mid)) + dot(upper, bf(low))
         decay_out[:, ks] = within + cross
 
-    settle(o_recv.at[0:15], o_sem, 1)
-    out_total = o_recv[0].astype(jnp.float32)
-    for n in range(1, 16):
-        out_total = out_total + o_recv[n].astype(jnp.float32)
-    out_out[...] = out_total
-    settle(o_recv.at[0:15], o_sem, 0)
+    settle(o_last.at[0:3], o2_sem, 1)
+    settle(p_last.at[0:3], p2_sem, 1)
+    out_out[:, :512] = total_of(o_last)
+    out_out[:, 512:] = total_of(p_last)
+    settle(o_recv.at[0:3], o_sem, 0)
+    settle(p_recv.at[0:3], p_sem, 0)
+    settle(o_last.at[0:3], o2_sem, 0)
+    settle(p_last.at[0:3], p2_sem, 0)
     settle(b_back.at[0:63], f_sem, 0)
 
 
@@ -655,11 +697,17 @@
         ((64, 16, 128), b16),
         ((1024, 128), b16),
         ((512, 512), b16),
-        ((512, 1024), b16),
-        ((16, 32, 1024), b16),
+        ((512, 512), b16),
+        ((4, 128, 512), b16),
+        ((128, 512), b16),
+        ((4, 32, 512), b16),
+        ((512, 512), b16),
+        ((4, 128, 512), b16),
+        ((128, 512), b16),
+        ((4, 32, 512), b16),
     )
     two, many = (2,), (CHUNKS, 2)
-    sems = [(10,), two] + [many] * 7 + [two] * 8
+    sems = [(10,), two] + [many] * 7 + [two] * 12
     made = pl.pallas_call(
         layer_kernel,
         name="whole_layer",

time: 102 us -> 95 us (0.931)
  Pallas kernels: 101 us -> 94.1 us
    pallas_call x1, Pallas kernels: 98.2 us -> 91.1 us  [whole_layer(): pl.pallas_call(layer_kernel, name='whole_layer', out_shape=tuple((v(shape...]
where the time goes in v3:
time: 95 us; the launch traced here: 94.9 us
  Pallas kernels  94.1 us (99%)
    pallas_call x1, Pallas kernels, whole_layer(): pl.pallas_call(layer_kernel, name='whole_layer', out_shape=tuple((v(shape...  91.1 us
    pallas_call x1, Pallas kernels, whole_layer(): pl.pallas_call(finish_kernel, name='finish', out_shape=tuple((jax.ShapeDt...  2.98 us

profile of v3, /device:TPU:1, one launch (start us, length us, event | category | flops | bytes accessed | tf_op | source)
XLA Modules:
  0.0 94.9 jit_solution(9493898728562381566)
XLA Ops:
  0.6 91.1 %whole_layer.1 = (bf16[1,2048,512]{2,1,0:T(8,128)(2,1)S(1)}, bf16[1,2048,512]{2,1,0:T(8,128)(2,1)S(1)}, bf16[1,512,2048]{2,1,0:T(8,128)(2,1)S(1)}, f32[32,1024]{...) custom-call(s32[2,64]{1,0:T(2,128)} %bitcast.2, ...), custom_call_target="tpu_custom_call" | custom-call | flops 11000000512 | bytes 20000000 | tf_op jit(solution)/shard_map/whole_layer/pallas_call | solution.py:711
  91.8 3.0 %finish.1 = (bf16[1,2048,512]{2,1,0:T(8,128)(2,1)}, bf16[1,2048,512]{2,1,0:T(8,128)(2,1)}, bf16[1,512,2048]{2,1,0:T(8,128)(2,1)}, f32[32,1024]{1,0:T(8,128)}, bf...) custom-call(bf16[1,2048,512]{2,1,0:T(8,128)(2,1)S(1)} %get-tuple-element.16.r, ...), custom_call_target="tpu_custom_call" | custom-call | tf_op jit(solution)/shard_map/finish/pallas_call | solution.py:725

commit v4 on v3

--- a/solution.py
+++ b/solution.py
@@ -90,6 +90,40 @@
 )
 CHUNKS = 4
 WIDE = 2048 // CHUNKS
+ORDER = [4 * place + c for c in range(CHUNKS) for place in range(4)]
+BOUNDS = (0, 2, 6, 10, 14, 16)
+STEPS = tuple(zip(BOUNDS[:-1], BOUNDS[1:]))
+LANES = 128
+
+
+def block_of(p):
+    return slice(ORDER[p] * LANES, (ORDER[p] + 1) * LANES)
+
+
+def taken_columns(ref, low, high):
+    return jnp.concatenate([ref[:, block_of(p)] for p in range(low, high)], axis=1)
+
+
+def taken_rows(ref, low, high):
+    return jnp.concatenate([ref[block_of(p), :] for p in range(low, high)], axis=0)
+
+
+def mid_part(low, high):
+    return slice(2 * low * LANES, (low + high) * LANES)
+
+
+def cot_part_of(low, high):
+    return slice((low + high) * LANES, 2 * high * LANES)
+
+
+def both_parts(low, high):
+    return slice(2 * low * LANES, 2 * high * LANES)
+
+
+def cot_block(p):
+    low, high = [step for step in STEPS if step[0] <= p < step[1]][0]
+    at = low + high + p - low
+    return slice(at * LANES, (at + 1) * LANES)
 
 
 def layer_kernel(
@@ -274,10 +308,9 @@
     loads[0].wait()
     loads[1].wait()
 
-    def fill_z(c):
-        cut = slice(c * WIDE, (c + 1) * WIDE)
-        z_send[c, :, :WIDE] = bf(dot(z_pick, mid_ref[:, cut]))
-        z_send[c, :, WIDE:] = bf(dot(z_pick, cot_ref[:, cut]))
+    def fill_z(n):
+        z_send[:, mid_part(*STEPS[n])] = bf(dot(z_pick, taken_columns(mid_ref, *STEPS[n])))
+        z_send[:, cot_part_of(*STEPS[n])] = bf(dot(z_pick, taken_columns(cot_ref, *STEPS[n])))
 
     fill_z(0)
     pl.semaphore_wait(barrier, len(peers))
@@ -287,13 +320,16 @@
         remote(z_note_send.at[there], z_note.at[own_z], n_sem, z_peer(dz))
     z_note[own_z, :] = z_note_send[own_z, :]
 
-    def send_z(c):
+    def send_z(n):
+        part = both_parts(*STEPS[n])
         for dz in (2, 1, 3):
             there = rows_at(ring(z, dz) * 32, 32)
-            remote(z_send.at[c, there], z_recv.at[c, own_z], z_sem.at[c], z_peer(dz))
-        z_recv[c, own_z, :] = z_send[c, own_z, :]
+            remote(z_send.at[there, part], z_recv.at[own_z, part], z_sem.at[n], z_peer(dz))
+        z_recv[own_z, part] = z_send[own_z, part]
 
     send_z(0)
+    fill_z(1)
+    send_z(1)
 
     along_z, along_y, along_x = [[ring(a, d) for d in range(4)] for a in (z, y, x)]
     bases = [[along_z[i] * 16 + along_y[j] * 4 for j in range(4)] for i in range(4)]
@@ -350,9 +386,9 @@
     all_to_all(state_out)
     s_recv[me] = s_send[own_state, :]
     d_recv[me] = d_send[me // 16]
-    for c in range(1, CHUNKS):
-        fill_z(c)
-        send_z(c)
+    for n in range(2, len(STEPS)):
+        fill_z(n)
+        send_z(n)
     got = z_note[...].astype(jnp.float32)
     token_row = lax.broadcasted_iota(jnp.int32, (128, 1), 0)
     offset = lax.shift_right_logical(token_row, 5) * 4
@@ -366,22 +402,23 @@
     weight_a = got[:, 2:3] + got[:, 3:4] + got[:, 4:5]
     weight_b = got[:, 5:6] + got[:, 6:7] + got[:, 7:8]
 
-    for c in range(CHUNKS):
-        settle(z_recv.at[c, 0:96], z_sem.at[c], 1)
-        x_send[c, :, :WIDE] = bf(dot_rows(place, z_recv[c, :, :WIDE]))
-        cot_part = z_recv[c, :, WIDE:].astype(jnp.float32)
-        x_send[c, :, WIDE:] = bf(
+    for c, step in enumerate(STEPS):
+        settle(z_recv.at[0:96, both_parts(*step)], z_sem.at[c], 1)
+        x_send[:, mid_part(*step)] = bf(dot_rows(place, z_recv[:, mid_part(*step)]))
+        cot_part = z_recv[:, cot_part_of(*step)].astype(jnp.float32)
+        x_send[:, cot_part_of(*step)] = bf(
             dot_rows(place_a, bf(weight_a * cot_part)) + dot_rows(place_b, bf(weight_b * cot_part))
         )
+        part = both_parts(*step)
         for dy, dx in PLANE:
             there = rows_at((ring(y, dy) * 4 + ring(x, dx)) * 16, 16)
             remote(
-                x_send.at[c, there],
-                rows.at[c, rows_at(mine + here * 16, 16)],
+                x_send.at[there, part],
+                rows.at[rows_at(mine + here * 16, 16), part],
                 x_sem.at[c],
                 plane_peer(dy, dx),
             )
-        rows[c, rows_at(mine + here * 16, 16), :] = x_send[c, own_x, :]
+        rows[rows_at(mine + here * 16, 16), part] = x_send[own_x, part]
         if c == 1:
             settle(s_recv.at[0:63], s_sem, 1)
             settle(d_recv.at[0:63], e_sem, 1)
@@ -418,19 +455,21 @@
     own_rows = rows_at(mine, 256)
 
     def gather_up(c, part):
-        cut = slice(c * WIDE, (c + 1) * WIDE)
+        step = STEPS[c]
+        mid_rows = rows[part, mid_part(*step)]
         for ref, value in (
-            (pre_gate, dot(rows[c, part, :WIDE], gate_w[cut, :])),
-            (pre_up, dot(rows[c, part, :WIDE], up_w[cut, :])),
-            (back_hidden, dot_cols(rows[c, part, WIDE:], down_w[:, cut])),
+            (pre_gate, dot(mid_rows, taken_rows(gate_w, *step))),
+            (pre_up, dot(mid_rows, taken_rows(up_w, *step))),
+            (back_hidden, dot_cols(rows[part, cot_part_of(*step)], taken_columns(down_w, *step))),
         ):
             ref[part, :] = value if c == 0 else ref[part, :] + value
 
-    for c in range(CHUNKS):
-        settle(rows.at[c, 0:240], x_sem.at[c], 1)
-        remote(rows.at[c, own_rows], rows.at[c, own_rows], d_sem.at[c], partner)
+    for c, step in enumerate(STEPS):
+        part = both_parts(*step)
+        settle(rows.at[0:240, part], x_sem.at[c], 1)
+        remote(rows.at[own_rows, part], rows.at[own_rows, part], d_sem.at[c], partner)
         gather_up(c, own_rows)
-        settle(rows.at[c, 0:256], d_sem.at[c], 1)
+        settle(rows.at[0:256, part], d_sem.at[c], 1)
         gather_up(c, their_rows)
 
     gate_swish, gate_slope = silu_parts(pre_gate[...])
@@ -439,9 +478,9 @@
     back_up[...] = bf(back_hidden[...] * gate_swish)
 
     def half_of(part, c):
-        cut = slice(c * WIDE, (c + 1) * WIDE)
         return bf(
-            dot_cols(back_gate[part, :], gate_w[cut, :]) + dot_cols(back_up[part, :], up_w[cut, :])
+            dot_cols(back_gate[part, :], taken_rows(gate_w, 4 * c, 4 * c + 4))
+            + dot_cols(back_up[part, :], taken_rows(up_w, 4 * c, 4 * c + 4))
         )
 
     def send_half(c):
@@ -463,17 +502,24 @@
             send_half(c + 1)
         give_back(c)
 
-    for c in range(CHUNKS):
-        cut = slice(c * WIDE, (c + 1) * WIDE)
-        gate_out[0, cut, :] = bf(dot_rows(rows[c, :, :WIDE], back_gate[...]))
-        up_out[0, cut, :] = bf(dot_rows(rows[c, :, :WIDE], back_up[...]))
-        down_out[0, :, cut] = bf(dot_rows(hidden[...], rows[c, :, WIDE:]))
+    for low, high in STEPS:
+        mid_rows = rows[:, mid_part(low, high)]
+        for out, grad in ((gate_out, back_gate), (up_out, back_up)):
+            value = bf(dot_rows(mid_rows, grad[...]))
+            for p in range(low, high):
+                out[0, block_of(p), :] = value[(p - low) * LANES : (p - low + 1) * LANES, :]
+        value = bf(dot_rows(hidden[...], rows[:, cot_part_of(low, high)]))
+        for p in range(low, high):
+            down_out[0, :, block_of(p)] = value[:, (p - low) * LANES : (p - low + 1) * LANES]
 
     own_tokens = rows_at(tp * 64, 64)
 
     def to_tokens(c):
         settle(ret_recv.at[c, 0:240], r_sem.at[c], 1)
-        tok_send[c] = bf(z_recv[c, :, WIDE:].astype(jnp.float32) + dot(place, ret_recv[c]))
+        cot_rows = jnp.concatenate(
+            [z_recv[:, cot_block(p)] for p in range(4 * c, 4 * c + 4)], axis=1
+        )
+        tok_send[c] = bf(cot_rows.astype(jnp.float32) + dot(place, ret_recv[c]))
         for dz in (2, 1, 3):
             there = rows_at(ring(z, dz) * 32, 32)
             remote(tok_send.at[c, there], tok_recv.at[c, own_z], t_sem.at[c], z_peer(dz))
@@ -484,14 +530,17 @@
         token_all[c, own_tokens, :] = bf(dot_rows(z_pick, tok_recv[c]))
         part = token_all.at[c, own_tokens]
         remote(part, part, a_sem.at[c], partner)
-
-        @pl.when(z != c)
-        def send():
-            remote(part, tz.at[rows_at(z * 128 + tp * 64, 64)], tz_sem, (c, y, x, tp))
+        for d in (2, 1, 3):
+            remote(
+                token_all.at[c, own_tokens, rows_at(along_z[d] * LANES, LANES)],
+                tz.at[rows_at(z * 128 + tp * 64, 64), c * LANES : (c + 1) * LANES],
+                tz_sem,
+                z_peer(d),
+            )
 
     def use_tokens(c, total):
         settle(token_all.at[c, 0:64], a_sem.at[c], 1)
-        value = dot(token_all[c], out_w[c * WIDE : (c + 1) * WIDE, :])
+        value = dot(token_all[c], taken_rows(out_w, 4 * c, 4 * c + 4))
         return value if total is None else total + value
 
     to_tokens(0)
@@ -520,7 +569,10 @@
     all_to_all(grad_out)
     b_recv[me] = b_send[own_state, :]
 
-    tz[rows_at(z * 128, 128), :] = token_all[z]
+    for c in range(CHUNKS):
+        tz[rows_at(z * 128, 128), c * LANES : (c + 1) * LANES] = token_all[
+            c, :, rows_at(z * LANES, LANES)
+        ]
     settle(tz.at[0:192], tz_sem, 1)
     for d in (1, 2, 3):
         part = tz.at[rows_at(along_z[d] * 128 + tp * 64, 64)]
@@ -581,10 +633,11 @@
     settle(tz.at[0:192], tz_sem, 0)
     settle(tz.at[0:192], tz2_sem, 0)
     settle(b_send.at[0:1008], b_sem, 0)
+    for c, step in enumerate(STEPS):
+        settle(z_send.at[0:96, both_parts(*step)], z_sem.at[c], 0)
+        settle(x_send.at[0:240, both_parts(*step)], x_sem.at[c], 0)
+        settle(rows.at[0:256, both_parts(*step)], d_sem.at[c], 0)
     for c in range(CHUNKS):
-        settle(z_send.at[c, 0:96], z_sem.at[c], 0)
-        settle(x_send.at[c, 0:240], x_sem.at[c], 0)
-        settle(rows.at[c, 0:256], d_sem.at[c], 0)
         settle(half_send.at[c], h_sem.at[c], 0)
         settle(ret_send.at[c, 0:240], r_sem.at[c], 0)
         settle(tok_send.at[c, 0:96], t_sem.at[c], 0)
@@ -656,12 +709,12 @@
         ((128, 512), b16),
         ((128, 1024), b16),
         ((128, 512), f32),
-        ((CHUNKS, 128, 2 * WIDE), b16),
+        ((128, 4096), b16),
         ((128, 128), b16),
-        ((CHUNKS, 128, 2 * WIDE), b16),
+        ((128, 4096), b16),
         ((128, 128), b16),
-        ((CHUNKS, 256, 2 * WIDE), b16),
-        ((CHUNKS, 512, 2 * WIDE), b16),
+        ((256, 4096), b16),
+        ((512, 4096), b16),
         ((512, 512), f32),
         ((512, 512), f32),
         ((512, 512), f32),
@@ -706,8 +759,8 @@
         ((128, 512), b16),
         ((4, 32, 512), b16),
     )
-    two, many = (2,), (CHUNKS, 2)
-    sems = [(10,), two] + [many] * 7 + [two] * 12
+    two, many, steps = (2,), (CHUNKS, 2), (len(STEPS), 2)
+    sems = [(10,), two] + [steps] * 3 + [many] * 4 + [two] * 12
     made = pl.pallas_call(
         layer_kernel,
         name="whole_layer",

time: 95 us -> 91.1 us (0.959)
  Pallas kernels: 94.1 us -> 90.2 us
    pallas_call x1, Pallas kernels: 91.1 us -> 87.2 us  [whole_layer(): pl.pallas_call(layer_kernel, name='whole_layer', out_shape=tuple((v(shape...]
where the time goes in v4:
time: 91.1 us; the launch traced here: 91 us
  Pallas kernels  90.2 us (99%)
    pallas_call x1, Pallas kernels, whole_layer(): pl.pallas_call(layer_kernel, name='whole_layer', out_shape=tuple((v(shape...  87.2 us
    pallas_call x1, Pallas kernels, whole_layer(): pl.pallas_call(finish_kernel, name='finish', out_shape=tuple((jax.ShapeDt...  2.98 us

profile of v4, /device:TPU:1, one launch (start us, length us, event | category | flops | bytes accessed | tf_op | source)
XLA Modules:
  0.0 91.0 jit_solution(9591217733990162218)
XLA Ops:
  0.6 87.2 %whole_layer.1 = (bf16[1,2048,512]{2,1,0:T(8,128)(2,1)S(1)}, bf16[1,2048,512]{2,1,0:T(8,128)(2,1)S(1)}, bf16[1,512,2048]{2,1,0:T(8,128)(2,1)S(1)}, f32[32,1024]{...) custom-call(s32[2,64]{1,0:T(2,128)} %bitcast.2, ...), custom_call_target="tpu_custom_call" | custom-call | flops 11000000512 | bytes 20000000 | tf_op jit(solution)/shard_map/whole_layer/pallas_call | solution.py:764
  87.9 3.0 %finish.1 = (bf16[1,2048,512]{2,1,0:T(8,128)(2,1)}, bf16[1,2048,512]{2,1,0:T(8,128)(2,1)}, bf16[1,512,2048]{2,1,0:T(8,128)(2,1)}, f32[32,1024]{1,0:T(8,128)}, bf...) custom-call(bf16[1,2048,512]{2,1,0:T(8,128)(2,1)S(1)} %get-tuple-element.16.r, ...), custom_call_target="tpu_custom_call" | custom-call | tf_op jit(solution)/shard_map/finish/pallas_call | solution.py:778

commit v5 on v4

--- a/solution.py
+++ b/solution.py
@@ -223,6 +223,7 @@
     nz_sem,
     tz_sem,
     tz2_sem,
+    tz3_sem,
     o_sem,
     o2_sem,
     p_sem,
@@ -530,13 +531,15 @@
         token_all[c, own_tokens, :] = bf(dot_rows(z_pick, tok_recv[c]))
         part = token_all.at[c, own_tokens]
         remote(part, part, a_sem.at[c], partner)
+        last = c == CHUNKS - 1
         for d in (2, 1, 3):
-            remote(
-                token_all.at[c, own_tokens, rows_at(along_z[d] * LANES, LANES)],
-                tz.at[rows_at(z * 128 + tp * 64, 64), c * LANES : (c + 1) * LANES],
-                tz_sem,
-                z_peer(d),
-            )
+            for core in (tp, other) if last else (tp,):
+                remote(
+                    token_all.at[c, own_tokens, rows_at(along_z[d] * LANES, LANES)],
+                    tz.at[rows_at(z * 128 + tp * 64, 64), c * LANES : (c + 1) * LANES],
+                    tz3_sem if last else tz_sem,
+                    (along_z[d], y, x, core),
+                )
 
     def use_tokens(c, total):
         settle(token_all.at[c, 0:64], a_sem.at[c], 1)
@@ -554,6 +557,10 @@
     back_normed = use_tokens(1, back_normed)
     share_tokens(3)
     back_normed = use_tokens(2, back_normed)
+    settle(tz.at[0:192, 0:384], tz_sem, 1)
+    for d in (1, 2, 3):
+        part = tz.at[rows_at(along_z[d] * 128 + tp * 64, 64), 0:384]
+        remote(part, part, tz2_sem, partner)
     back_normed = use_tokens(3, back_normed)
 
     for h in range(4):
@@ -573,11 +580,8 @@
         tz[rows_at(z * 128, 128), c * LANES : (c + 1) * LANES] = token_all[
             c, :, rows_at(z * LANES, LANES)
         ]
-    settle(tz.at[0:192], tz_sem, 1)
-    for d in (1, 2, 3):
-        part = tz.at[rows_at(along_z[d] * 128 + tp * 64, 64)]
-        remote(part, part, tz2_sem, partner)
-    settle(tz.at[0:192], tz2_sem, 1)
+    settle(tz.at[0:192, 0:384], tz2_sem, 1)
+    settle(tz.at[0:384, 384:512], tz3_sem, 1)
     settle(n_all.at[0:384], nz_sem, 1)
     o_send[...] = bf(dot_rows(tz[...], n_all[:, :512]))
     for d in (2, 1, 3):
@@ -630,8 +634,9 @@
     settle(d_recv.at[0:63], e_sem, 0)
     settle(s_back.at[0:63], i_sem, 0)
     settle(n_all.at[0:384], nz_sem, 0)
-    settle(tz.at[0:192], tz_sem, 0)
-    settle(tz.at[0:192], tz2_sem, 0)
+    settle(tz.at[0:192, 0:384], tz_sem, 0)
+    settle(tz.at[0:192, 0:384], tz2_sem, 0)
+    settle(tz.at[0:384, 384:512], tz3_sem, 0)
     settle(b_send.at[0:1008], b_sem, 0)
     for c, step in enumerate(STEPS):
         settle(z_send.at[0:96, both_parts(*step)], z_sem.at[c], 0)
@@ -760,7 +765,7 @@
         ((4, 32, 512), b16),
     )
     two, many, steps = (2,), (CHUNKS, 2), (len(STEPS), 2)
-    sems = [(10,), two] + [steps] * 3 + [many] * 4 + [two] * 12
+    sems = [(10,), two] + [steps] * 3 + [many] * 4 + [two] * 13
     made = pl.pallas_call(
         layer_kernel,
         name="whole_layer",

time: 91.1 us -> 90.6 us (level)
  no operation moved by 1% of the time
where the time goes in v5:
time: 90.6 us; the launch traced here: 90.4 us
  Pallas kernels  89.6 us (99%)
    pallas_call x1, Pallas kernels, whole_layer(): pl.pallas_call(layer_kernel, name='whole_layer', out_shape=tuple((v(shape...  86.6 us
    pallas_call x1, Pallas kernels, whole_layer(): pl.pallas_call(finish_kernel, name='finish', out_shape=tuple((jax.ShapeDt...  2.98 us

profile of v5, /device:TPU:1, one launch (start us, length us, event | category | flops | bytes accessed | tf_op | source)
XLA Modules:
  0.0 90.4 jit_solution(14516103743594505604)
XLA Ops:
  0.6 86.6 %whole_layer.1 = (bf16[1,2048,512]{2,1,0:T(8,128)(2,1)S(1)}, bf16[1,2048,512]{2,1,0:T(8,128)(2,1)S(1)}, bf16[1,512,2048]{2,1,0:T(8,128)(2,1)S(1)}, f32[32,1024]{...) custom-call(s32[2,64]{1,0:T(2,128)} %bitcast.2, ...), custom_call_target="tpu_custom_call" | custom-call | flops 11000000512 | bytes 20000000 | tf_op jit(solution)/shard_map/whole_layer/pallas_call | solution.py:769
  87.3 3.0 %finish.1 = (bf16[1,2048,512]{2,1,0:T(8,128)(2,1)}, bf16[1,2048,512]{2,1,0:T(8,128)(2,1)}, bf16[1,512,2048]{2,1,0:T(8,128)(2,1)}, f32[32,1024]{1,0:T(8,128)}, bf...) custom-call(bf16[1,2048,512]{2,1,0:T(8,128)(2,1)S(1)} %get-tuple-element.16.r, ...), custom_call_target="tpu_custom_call" | custom-call | tf_op jit(solution)/shard_map/finish/pallas_call | solution.py:783
